TPU v7x, 256 devices: a whole 4x4x8 slice. The times are simulated.
256 devices in a mesh: sp: 16 (over y, x), tp: 16 (over z, core).
Axes of the slice: x: 4, y: 4, z: 8, core: 2. Of those that a mesh axis runs over, the one named last changes fastest.
Arguments:
- queries: bfloat16 [32768, 2048], P('sp', 'tp'), may hold values from -160 to 160
- key_heads: bfloat16 [32768, 512], P('sp'), may hold values from -8 to 8
- value_heads: bfloat16 [32768, 512], P('sp'), may hold values from -4 to 4
- sink_logit: float32 [16], P('tp'), may hold values from -2 to 7
- out_weight: bfloat16 [2048, 2048], P('tp'), may hold values from -0.125 to 0.125
- residual: bfloat16 [32768, 2048], P(('sp', 'tp')), may hold values from -6 to 6
- mixer_gain: float32 [2048], replicated, may hold values from 0.1 to 1.9
- expert_gain: float32 [2048], replicated, may hold values from 0.1 to 1.9
- route_group: int32 [32768], P(('sp', 'tp')), may hold values from 0 to 15, as said below
- route_member: int32 [32768, 2], P(('sp', 'tp')), may hold values from 0 to 2, as said below
- route_weight: bfloat16 [32768, 2], P(('sp', 'tp')), may hold values from 0.19921875 to 1
- gate_weight: bfloat16 [48, 2048, 2048], P('sp', None, 'tp'), may hold values from -0.125 to 0.125
- up_weight: bfloat16 [48, 2048, 2048], P('sp', None, 'tp'), may hold values from -0.125 to 0.125
- down_weight: bfloat16 [48, 2048, 2048], P('sp', 'tp'), may hold values from -0.125 to 0.125
Outputs:
- output: bfloat16 [32768, 2048], P(('sp', 'tp'))
Inputs may be any that keep to these rules, and one draw needn't show every extreme that they name: `route_group`: among the tokens of one device, at most 10 name one group; in every draw one group is named by exactly 10 tokens of every device. `route_member`: the two entries of a token are different members of its group.
All inputs are finite; a program needn't handle non-finite values.
Results may differ from a plain program's by a relative error of at most 0.018.
Values may be sent and summed in bfloat16 or wider, within the bound.
No kernel may reach another device: no remote copies, remote signals or barrier semaphores. Data moves between devices by JAX's collectives and lax.ppermute only.
A program may use at most 128 MiB of HBM per device.

v0:
```python
import jax
import jax.numpy as jnp
from jax import lax
from jax.experimental import pallas as pl
from jax.experimental.pallas import tpu as pltpu
from jax.sharding import Mesh
from jax.sharding import PartitionSpec as P


HEADS = 16
KV_HEADS = 4
HEAD_DIM = 128
WINDOW = 128
BLOCK = 128
GROUP_EXPERTS = 3
GROUP_CAP = 10
LANES = 128
Z = "tp_0"
CORE = "tp_1"
TP = (Z, CORE)
SP_TP = ("sp", Z, CORE)
SWAP = [(0, 1), (1, 0)]

EPS = 1e-06
NEG_BIG = -1e30


def extended(block, width):
    count = lax.axis_size("sp")
    forward = [(i, i + 1) for i in range(count - 1)]
    backward = [(target, source) for source, target in forward]
    low = lax.ppermute(block[:, block.shape[1] - width :], "sp", forward)
    high = lax.ppermute(block[:, :width], "sp", backward)
    return jnp.concatenate([low, block, high], axis=1)


def chip_attention(queries, key_heads, value_heads, sink_logit):
    seq_rows = queries.shape[0]
    core = lax.axis_index(CORE)
    key_start = lax.axis_index(Z) * 2 * KV_HEADS // HEADS * HEAD_DIM
    key_own = lax.dynamic_slice_in_dim(key_heads, key_start, HEAD_DIM, 1)
    value_own = lax.dynamic_slice_in_dim(value_heads, key_start, HEAD_DIM, 1)
    padded = extended(jnp.stack([key_own, value_own]), WINDOW)
    blocks = seq_rows // (2 * BLOCK)
    query_blocks = queries.reshape(blocks, 2, BLOCK, HEAD_DIM)
    query_far = lax.ppermute(
        lax.dynamic_index_in_dim(query_blocks, 1 - core, 1, True), CORE, SWAP
    )
    query_pair = jnp.concatenate(
        [lax.dynamic_index_in_dim(query_blocks, core, 1, True), query_far], axis=1
    )
    sink_pair = jnp.concatenate([sink_logit, lax.ppermute(sink_logit, CORE, SWAP)])
    tile_rows = padded.reshape(2, 2 * blocks + 2, BLOCK, HEAD_DIM)
    key_spans = jnp.concatenate(
        [
            lax.dynamic_slice_in_dim(tile_rows, core + shifted, 2 * blocks - 1, 1)[:, ::2]
            for shifted in range(3)
        ],
        axis=2,
    )
    offset = lax.axis_index("sp") * seq_rows
    seq_total = seq_rows * lax.axis_size("sp")
    block_start = offset + (2 * jnp.arange(blocks, dtype=jnp.int32) + core) * BLOCK
    query_pos = block_start[:, None] + jnp.arange(BLOCK, dtype=jnp.int32)[None, :]
    key_pos = (
        block_start[:, None] + jnp.arange(BLOCK + 2 * WINDOW, dtype=jnp.int32)[None, :] - WINDOW
    )
    inside = (
        (jnp.abs(query_pos[:, :, None] - key_pos[:, None, :]) <= WINDOW)
        & (key_pos >= 0)[:, None, :]
        & (key_pos < seq_total)[:, None, :]
    )
    scores = jnp.einsum(
        "nhqd,nkd->nhqk", query_pair, key_spans[0], preferred_element_type=jnp.float32
    ) * HEAD_DIM ** (-0.5)
    scores = jnp.where(inside[:, None], scores, NEG_BIG)
    sink_col = sink_pair[None, :, None, None]
    row_top = jnp.maximum(jnp.max(scores, axis=3, keepdims=True), sink_col)
    exp_terms = jnp.exp(scores - row_top)
    row_mass = jnp.sum(exp_terms, axis=3, keepdims=True) + jnp.exp(sink_col - row_top)
    weight = (exp_terms / row_mass).astype(jnp.bfloat16)
    return jnp.einsum(
        "nhqk,nkd->nhqd", weight, key_spans[1], preferred_element_type=jnp.float32
    ).astype(jnp.bfloat16)


MAIN_CAP = 7
MAIN_COLS = 1280
REL = (0, -1, 1, -2, 2, -3, 3, 4)


def shifts():
    n = lax.axis_size(Z)
    up = [(i, (i + 1) % n) for i in range(n)]
    down = [(i, (i - 1) % n) for i in range(n)]
    return (lambda a: lax.ppermute(a, Z, up)), (lambda a: lax.ppermute(a, Z, down))


def ring_gather(block):
    up, down = shifts()
    half = block.shape[1] // (2 * LANES) * LANES
    blocks, low, high = [block], block, block
    for _ in range(3):
        low, high = up(low), down(high)
        blocks += [low, high]
    far = jnp.concatenate([up(low[:, :half]), down(high[:, half:])], axis=1)
    return blocks + [far]


def ring_reduce(parts):
    up, down = shifts()
    half = parts[0].shape[1] // 2
    low, high = up(parts[4][:, :half]), down(parts[4][:, half:])
    low = jnp.concatenate([parts[3][:, :half] + low, parts[3][:, half:]], axis=1)
    high = jnp.concatenate([parts[-3][:, :half], parts[-3][:, half:] + high], axis=1)
    for step in (2, 1):
        low, high = parts[step] + up(low), parts[-step] + down(high)
    return parts[0] + up(low) + down(high)


def in_ring_order(blocks, near_first):
    me = lax.axis_index(Z)
    n = lax.axis_size(Z)
    return [lax.dynamic_index_in_dim(blocks, (me + r) % n, 0, False) for r in near_first]


def experts_kernel(rows_in, *refs):
    weights_in, out_to = refs[:6], refs[6]
    weights, (rows, hidden, out) = refs[7:13], refs[13:16]
    weight_sems, row_sems, out_sems = refs[16:]
    gate_own, gate_far, up_own, up_far, down_own, down_far = weights
    total = rows.shape[0]
    width = out.shape[1]
    hid = 2 * gate_own.shape[2]
    steps = -(-total // 512)
    step = total // steps
    wide = 512

    def span(i):
        return pl.ds(pl.multiple_of(i * step, 16), step)

    def weight_copy(k, e):
        return pltpu.make_async_copy(weights_in[k].at[e], weights[k].at[e], weight_sems.at[k, e])

    def row_copy(i):
        return pltpu.make_async_copy(rows_in.at[span(i)], rows.at[span(i)], row_sems.at[i])

    def out_copy(i):
        return pltpu.make_async_copy(out.at[span(i)], out_to.at[span(i)], out_sems.at[i])

    for k in range(4):
        weight_copy(k, 0).start()
    for i in range(steps):
        row_copy(i).start()
    for e in range(1, GROUP_EXPERTS):
        for k in range(4):
            weight_copy(k, e).start()
    for e in range(GROUP_EXPERTS):
        for k in (4, 5):
            weight_copy(k, e).start()

    @pl.loop(0, GROUP_EXPERTS)
    def _(e):
        for k in range(4):
            weight_copy(k, e).wait()

        @pl.loop(0, steps)
        def _(i):
            @pl.when(e == 0)
            def _():
                row_copy(i).wait()

            joined = jnp.concatenate([gate_own[e], gate_far[e], up_own[e], up_far[e]], axis=1)
            both = jnp.dot(rows[span(i), :width], joined, preferred_element_type=jnp.float32)
            pre = both[:, :hid]
            gates = rows[span(i), width:].astype(jnp.float32)
            lane = lax.broadcasted_iota(jnp.int32, gates.shape, 1)
            gate = jnp.sum(jnp.where(lane == e, gates, 0.0), axis=1, keepdims=True)
            gated = pre / (1.0 + jnp.exp(-pre)) * both[:, hid:] * gate
            hidden[e, span(i), :] = gated.astype(jnp.bfloat16)

    for e in range(GROUP_EXPERTS):
        for k in (4, 5):
            weight_copy(k, e).wait()

    @pl.loop(0, steps)
    def _(i):
        joined = jnp.concatenate([hidden[e, span(i), :] for e in range(GROUP_EXPERTS)], axis=1)

        @pl.loop(0, width // wide)
        def _(c):
            cols = pl.ds(pl.multiple_of(c * wide, wide), wide)
            pieces = []
            for e in range(GROUP_EXPERTS):
                pieces += [down_own[e, :, cols], down_far[e, :, cols]]
            out[span(i), cols] = jnp.dot(
                joined, jnp.concatenate(pieces, axis=0), preferred_element_type=jnp.float32
            ).astype(jnp.bfloat16)

        out_copy(i).start()

    for i in range(steps):
        out_copy(i).wait()


def experts(rows, gate_pair, up_pair, down_pair):
    total, lanes = rows.shape
    width = lanes - LANES
    hid = gate_pair[0].shape[2]
    steps = -(-total // 512)
    work = total * width * hid * 2 * GROUP_EXPERTS
    anywhere = pl.BlockSpec(memory_space=pltpu.HBM)
    into = pltpu.VMEM((GROUP_EXPERTS, width, hid), jnp.bfloat16)
    outof = pltpu.VMEM((GROUP_EXPERTS, hid, width), jnp.bfloat16)
    return pl.pallas_call(
        experts_kernel,
        in_specs=[anywhere] * 7,
        out_specs=anywhere,
        out_shape=jax.ShapeDtypeStruct((total, width), jnp.bfloat16),
        scratch_shapes=[into] * 4
        + [outof] * 2
        + [
            pltpu.VMEM((total, lanes), jnp.bfloat16),
            pltpu.VMEM((GROUP_EXPERTS, total, 2 * hid), jnp.bfloat16),
            pltpu.VMEM((total, width), jnp.bfloat16),
            pltpu.SemaphoreType.DMA((6, GROUP_EXPERTS)),
            pltpu.SemaphoreType.DMA((steps,)),
            pltpu.SemaphoreType.DMA((steps,)),
        ],
        compiler_params=pltpu.CompilerParams(vmem_limit_bytes=62 * 2**20),
        cost_estimate=pl.CostEstimate(
            flops=6 * work, bytes_accessed=20 * 2**20, transcendentals=total * hid * 6
        ),
        name="experts",
    )(rows, *gate_pair, *up_pair, *down_pair)


def per_device(
    queries,
    key_heads,
    value_heads,
    sink_logit,
    out_weight,
    residual,
    mixer_gain,
    expert_gain,
    route_group,
    route_member,
    route_weight,
    gate_weight,
    up_weight,
    down_weight,
):
    groups = lax.axis_size("sp")
    width = residual.shape[1]
    capacity = GROUP_CAP
    slots = groups * capacity
    cap_a = MAIN_CAP
    cap_b = capacity - cap_a
    slots_b = groups * cap_b


    gate_pair, up_pair, down_pair = (
        (shard, lax.ppermute(shard, CORE, SWAP))
        for shard in (gate_weight, up_weight, down_weight)
    )

    group_ids = jnp.arange(groups, dtype=jnp.int32)
    chosen = (route_group[:, None] == group_ids[None, :]).astype(jnp.int32)
    group_rank = jnp.sum(chosen * (jnp.cumsum(chosen, axis=0) - 1), axis=1)
    slot_ids = route_group * capacity + group_rank
    placing = (jnp.arange(slots, dtype=jnp.int32)[:, None] == slot_ids[None, :]).astype(
        jnp.bfloat16
    )
    member_ids = jnp.arange(GROUP_EXPERTS, dtype=jnp.int32)
    token_gates = jnp.sum(
        route_weight.astype(jnp.float32)[:, :, None]
        * (route_member[:, :, None] == member_ids[None, None, :]).astype(jnp.float32),
        axis=1,
    ).astype(jnp.bfloat16)
    send_gates = jnp.dot(
        placing,
        jnp.pad(token_gates, ((0, 0), (0, LANES - GROUP_EXPERTS))),
        preferred_element_type=jnp.float32,
    ).astype(jnp.bfloat16)
    send_gates = jnp.pad(
        send_gates.reshape(groups, capacity, LANES), ((0, 0), (0, 16 - capacity), (0, 0))
    )

    weight_pair = jnp.stack([out_weight, lax.ppermute(out_weight, CORE, SWAP)])
    attended = chip_attention(queries, key_heads, value_heads, sink_logit)

    def head_part(cols):
        return jnp.einsum(
            "nhqd,hdm->nqm", attended, weight_pair[:, :, cols], preferred_element_type=jnp.float32
        ).astype(jnp.bfloat16)

    ring_part = head_part(slice(MAIN_COLS, width))
    main_part = head_part(slice(0, MAIN_COLS)).reshape(-1, MAIN_COLS)
    main_sum = lax.psum_scatter(main_part, Z, scatter_dimension=0, tiled=True)
    ring_sum = ring_reduce(dict(zip(REL, in_ring_order(ring_part, REL))))
    projected = jnp.concatenate([main_sum, ring_sum], axis=1).astype(jnp.float32)
    projected, gate_pair, up_pair, down_pair = lax.optimization_barrier(
        (projected, gate_pair, up_pair, down_pair)
    )

    proj_scale = lax.rsqrt(jnp.mean(projected * projected, axis=1, keepdims=True) + EPS)
    mixed_rows = (residual.astype(jnp.float32) + mixer_gain * (projected * proj_scale)).astype(
        jnp.bfloat16
    )
    mixed_float = mixed_rows.astype(jnp.float32)
    norm_scale = lax.rsqrt(jnp.mean(mixed_float * mixed_float, axis=1, keepdims=True) + EPS)
    normed = (mixed_float * norm_scale * expert_gain).astype(jnp.bfloat16)

    def exchange(rows):
        return lax.all_to_all(
            rows.reshape(groups, -1, LANES), "sp", split_axis=0, concat_axis=0, tiled=True
        )

    send_rows = jnp.dot(placing, normed, preferred_element_type=jnp.float32).astype(jnp.bfloat16)
    send_rows = send_rows.reshape(groups, capacity * width // LANES, LANES)
    tiles = width // LANES
    arrived = exchange(jnp.concatenate([send_rows, send_gates], axis=1))

    def with_gates(low, high):
        rows = arrived[:, low * tiles : high * tiles].reshape(-1, width)
        gates = arrived[:, capacity * tiles + low : capacity * tiles + high].reshape(-1, LANES)
        return jnp.concatenate([rows, gates], axis=1)

    pool_a = lax.all_gather(with_gates(0, cap_a), Z, axis=0, tiled=True)
    pool_b = ring_gather(with_gates(cap_a, capacity))
    part_b = experts(jnp.concatenate(pool_b, axis=0), gate_pair, up_pair, down_pair)
    pool_a, part_b = lax.optimization_barrier((pool_a, part_b))
    part_a = experts(pool_a, gate_pair, up_pair, down_pair)
    sum_a = lax.psum_scatter(part_a, Z, scatter_dimension=0, tiled=True)
    sum_b = ring_reduce(
        {r: part_b[k * slots_b : (k + 1) * slots_b] for k, r in enumerate(REL)}
    )
    back_b = exchange(sum_b)
    back_a = exchange(sum_a)
    returned = jnp.concatenate([back_a, back_b], axis=1).reshape(slots, width)
    expert_out = lax.dot_general(
        placing,
        returned,
        (((0,), (0,)), ((), ())),
        preferred_element_type=jnp.float32,
    )
    return (mixed_float + expert_out).astype(jnp.bfloat16)


def solution(mesh):
    torus = Mesh(mesh.devices.reshape(mesh.shape["sp"], 8, 2), ("sp", Z, CORE))
    placed = (
        P("sp", TP),
        P("sp", None),
        P("sp", None),
        P(TP),
        P(TP, None),
        P(SP_TP, None),
        P(),
        P(),
        P(SP_TP),
        P(SP_TP, None),
        P(SP_TP, None),
        P("sp", None, TP),
        P("sp", None, TP),
        P("sp", TP, None),
    )

    return jax.shard_map(
        per_device, mesh=torus, in_specs=placed, out_specs=P(SP_TP, None), check_vma=False
    )
```

profile of v0, /device:TPU:96, one launch (start us, length us, event | category | flops | bytes accessed | tf_op | source)
XLA Modules:
  0.0 267.3 jit_solution(5375935818207105465)
XLA Ops:
  6.5 1.4 dynamic-slice_bitcast_fusion
  7.9 1.3 collective-permute-start.2
  9.2 4.5 %collective-permute-start.1 = (bf16[2,128,128]{2,1,0:T(8,128)(2,1)S(1)}, bf16[2,128,128]{2,1,0:T(8,128)(2,1)S(1)}, u32[]{:S(2)}, u32[]{:S(2)}) collective-permute-start(bf16[2,128,128]{2,1,0:T(8,128)(2,1)S(1)} %get-tuple-element.39), channel_id=1, source_target_pairs={{0,16},{16,32},{32,48},{48,64},{64,80},{80,96},{96,112},{112,128},... | collective-permute-start | bytes 196616 | tf_op jit(solution)/shard_map/ppermute | solution.py:32
  15.4 0.6 fusion.4
  16.1 0.7 pad_maximum_fusion.11
  17.4 0.9 fusion
  18.4 1.3 fusion.2
  19.7 1.3 fusion.7
  21.1 2.3 bitcast_convert_fusion
  24.5 0.6 bitcast_convert_fusion.1
  25.2 3.2 %collective-permute-start.5 = (bf16[128,384]{1,0:T(8,128)(2,1)S(1)}, bf16[128,384]{1,0:T(8,128)(2,1)S(1)}, u32[]{:S(2)}, u32[]{:S(2)}) collective-permute-start(bf16[128,384]{1,0:T(8,128)(2,1)S(1)} %get-tuple-element.47), channel_id=1, source_target_pairs={{0,2},{2,4},{4,6},{6,8},{8,10},{10,12},{12,14},{14,0},{1,3},{3,5},... | collective-permute-start | bytes 294920 | tf_op jit(solution)/shard_map/ppermute | solution.py:96
  28.6 2.1 collective-permute-done.5
  30.8 3.8 %collective-permute-start.6 = (bf16[128,768]{1,0:T(8,128)(2,1)S(1)}, bf16[128,768]{1,0:T(8,128)(2,1)S(1)}, u32[]{:S(2)}, u32[]{:S(2)}) collective-permute-start(bf16[128,768]{1,0:T(8,128)(2,1)S(1)} %pad_maximum_fusion.5), channel_id=1, source_target_pairs={{0,2},{2,4},{4,6},{6,8},{8,10},{10,12},{12,14},{14,0},{1,3},{3,5},... | collective-permute-start | bytes 589832 | tf_op jit(solution)/shard_map/ppermute | solution.py:96
  34.9 3.3 %collective-permute-done.6 = bf16[128,768]{1,0:T(8,128)(2,1)S(1)} collective-permute-done((bf16[128,768]{1,0:T(8,128)(2,1)S(1)}, bf16[128,768]{1,0:T(8,128)(2,1)S(1)}, u32[]{:S(2)}, u32[]{:S(2)}) %collective-permute-start.6) | collective-permute-done | bytes 196640 | tf_op jit(solution)/shard_map/ppermute | solution.py:96
  38.2 3.8 %collective-permute-start.7 = (bf16[128,768]{1,0:T(8,128)(2,1)S(1)}, bf16[128,768]{1,0:T(8,128)(2,1)S(1)}, u32[]{:S(2)}, u32[]{:S(2)}) collective-permute-start(bf16[128,768]{1,0:T(8,128)(2,1)S(1)} %bitcast_add_fusion.2), channel_id=1, source_target_pairs={{0,2},{2,4},{4,6},{6,8},{8,10},{10,12},{12,14},{14,0},{1,3},{3,5},... | collective-permute-start | bytes 589832 | tf_op jit(solution)/shard_map/ppermute | solution.py:96
  42.4 7.4 %collective-permute-done.7 = bf16[128,768]{1,0:T(8,128)(2,1)S(1)} collective-permute-done((bf16[128,768]{1,0:T(8,128)(2,1)S(1)}, bf16[128,768]{1,0:T(8,128)(2,1)S(1)}, u32[]{:S(2)}, u32[]{:S(2)}) %collective-permute-start.7) | collective-permute-done | bytes 196640 | tf_op jit(solution)/shard_map/ppermute | solution.py:96
  49.9 3.8 %collective-permute-start.8 = (bf16[128,768]{1,0:T(8,128)(2,1)S(1)}, bf16[128,768]{1,0:T(8,128)(2,1)S(1)}, u32[]{:S(2)}, u32[]{:S(2)}) collective-permute-start(bf16[128,768]{1,0:T(8,128)(2,1)S(1)} %get-tuple-element.31), channel_id=1, source_target_pairs={{0,2},{2,4},{4,6},{6,8},{8,10},{10,12},{12,14},{14,0},{1,3},{3,5},... | collective-permute-start | bytes 589832 | tf_op jit(solution)/shard_map/ppermute | solution.py:96
  53.7 8.5 %collective-permute-done.11 = bf16[128,768]{1,0:T(8,128)(2,1)S(1)} collective-permute-done((bf16[128,768]{1,0:T(8,128)(2,1)S(1)}, bf16[128,768]{1,0:T(8,128)(2,1)S(1)}, u32[]{:S(2)}, u32[]{:S(2)}) %collective-permute-start.11) | collective-permute-done | bytes 196640 | tf_op jit(solution)/shard_map/ppermute | solution.py:96
  62.5 11.3 %collective-permute-done.12 = bf16[128,768]{1,0:T(8,128)(2,1)S(1)} collective-permute-done((bf16[128,768]{1,0:T(8,128)(2,1)S(1)}, bf16[128,768]{1,0:T(8,128)(2,1)S(1)}, u32[]{:S(2)}, u32[]{:S(2)}) %collective-permute-start.12) | collective-permute-done | bytes 196640 | tf_op jit(solution)/shard_map/ppermute | solution.py:96
  73.8 5.2 %reduce-scatter.3.cloned.1.call-done = bf16[128,1280]{1,0:T(8,128)(2,1)} async-done(((bf16[1024,1280]{1,0:T(8,128)(2,1)}), bf16[128,1280]{1,0:T(8,128)(2,1)}) %reduce-scatter.3.cloned.1.call-update) | async-done | bytes 327696 | tf_op jit(solution)/shard_map/reduce_scatter | solution.py:300
  79.0 1.1 maximum_convert_fusion
  81.6 19.4 %all_to_all.15 = bf16[16,176,128]{2,1,0:T(8,128)(2,1)S(1)} all-to-all(bf16[16,176,128]{2,1,0:T(8,128)(2,1)S(1)} %fusion.12), channel_id=1, replica_groups=mesh['sp'=16,'tp_0'=8,'tp_1'=2] {'sp'}, dimensions={0} | all-to-all | bytes 1441792 | tf_op jit(solution)/shard_map/all_to_all | solution.py:316
  101.2 0.8 pad_maximum_fusion.3
  102.3 0.7 constant_dynamic-update-slice_fusion.1
  103.0 0.6 constant_dynamic-update-slice_fusion
  103.6 1.4 collective-permute-start.16
  105.1 0.6 collective-permute-start.17
  105.7 4.7 %collective-permute-done.16 = bf16[48,2176]{1,0:T(8,128)(2,1)S(1)} collective-permute-done((bf16[48,2176]{1,0:T(8,128)(2,1)S(1)}, bf16[48,2176]{1,0:T(8,128)(2,1)S(1)}, u32[]{:S(2)}, u32[]{:S(2)}) %collective-permute-start.16) | collective-permute-done | bytes 208928 | tf_op jit(solution)/shard_map/ppermute | solution.py:96
  110.4 1.7 collective-permute-start.18
  112.4 0.7 constant_dynamic-update-slice_fusion.7
  113.1 0.7 constant_dynamic-update-slice_fusion.6
  113.9 8.0 %collective-permute-done.18 = bf16[48,2176]{1,0:T(8,128)(2,1)S(1)} collective-permute-done((bf16[48,2176]{1,0:T(8,128)(2,1)S(1)}, bf16[48,2176]{1,0:T(8,128)(2,1)S(1)}, u32[]{:S(2)}, u32[]{:S(2)}) %collective-permute-start.18) | collective-permute-done | bytes 208928 | tf_op jit(solution)/shard_map/ppermute | solution.py:96
  121.8 2.7 collective-permute-start.20
  124.5 0.7 constant_dynamic-update-slice_fusion.5
  125.2 0.7 constant_dynamic-update-slice_fusion.4
  125.9 10.9 %collective-permute-done.21 = bf16[48,2176]{1,0:T(8,128)(2,1)S(1)} collective-permute-done((bf16[48,2176]{1,0:T(8,128)(2,1)S(1)}, bf16[48,2176]{1,0:T(8,128)(2,1)S(1)}, u32[]{:S(2)}, u32[]{:S(2)}) %collective-permute-start.21) | collective-permute-done | bytes 208928 | tf_op jit(solution)/shard_map/ppermute | solution.py:96
  137.0 3.5 %collective-permute-start.22 = (bf16[48,1024]{1,0:T(8,128)(2,1)S(1)}, bf16[48,1024]{1,0:T(8,128)(2,1)S(1)}, u32[]{:S(2)}, u32[]{:S(2)}) collective-permute-start(bf16[48,1024]{1,0:T(8,128)(2,1)S(1)} %slice.151), channel_id=1, source_target_pairs={{0,2},{2,4},{4,6},{6,8},{8,10},{10,12},{12,14},{14,0},{1,3},{3,5},... | collective-permute-start | bytes 294920 | tf_op jit(solution)/shard_map/ppermute | solution.py:96
  140.5 0.7 constant_dynamic-update-slice_fusion.3
  141.2 0.7 constant_dynamic-update-slice_fusion.2
  141.9 3.0 %collective-permute-done.22 = bf16[48,1024]{1,0:T(8,128)(2,1)S(1)} collective-permute-done((bf16[48,1024]{1,0:T(8,128)(2,1)S(1)}, bf16[48,1024]{1,0:T(8,128)(2,1)S(1)}, u32[]{:S(2)}, u32[]{:S(2)}) %collective-permute-start.22) | collective-permute-done | bytes 98336 | tf_op jit(solution)/shard_map/ppermute | solution.py:96
  144.8 0.5 collective-permute-done.23
  145.4 0.7 maximum_dynamic-update-slice_fusion.rows_in
  146.1 10.5 %experts.2 = bf16[384,2048]{1,0:T(8,128)(2,1)} custom-call(bf16[384,2176]{1,0:T(8,128)(2,1)} %maximum_dynamic-update-slice_fusion.rows_in, bf16[3,2048,128]{2,1,0:T(8,128)(2,1)} %refs_0_.1, bf16[3,2048,128]{2,1,0:T(8,128)(2,1)} %collective-permute-done.13.refs_1_, bf16[3,2048,128]{2,1,0:T(8,128)(2,1)} %refs_2_.1, ...), custom_call_target="tpu_custom_call" | custom-call | flops 3623878656 | bytes 20971520 | tf_op jit(solution)/shard_map/experts/pallas_call | solution.py:215
  156.6 4.4 %all-gather.2.cloned.1.call-done.rows_in = bf16[896,2176]{1,0:T(8,128)(2,1)} async-done(((bf16[112,2176]{1,0:T(8,128)(2,1)}), bf16[896,2176]{1,0:T(8,128)(2,1)}) %all-gather.2.cloned.1.call-update) | async-done | bytes 3899408 | tf_op jit(solution)/shard_map/all_gather | solution.py:330
  161.0 16.6 %experts.3 = bf16[896,2048]{1,0:T(8,128)(2,1)} custom-call(bf16[896,2176]{1,0:T(8,128)(2,1)} %all-gather.2.cloned.1.call-done.rows_in, bf16[3,2048,128]{2,1,0:T(8,128)(2,1)} %refs_0_.1, bf16[3,2048,128]{2,1,0:T(8,128)(2,1)} %collective-permute-done.13.refs_1_, bf16[3,2048,128]{2,1,0:T(8,128)(2,1)} %refs_2_.1, ...), custom_call_target="tpu_custom_call" | custom-call | flops 8455716864 | bytes 20971520 | tf_op jit(solution)/shard_map/experts/pallas_call | solution.py:215
  177.6 1.0 slice.130
  178.7 4.6 %collective-permute-done.24 = bf16[48,1024]{1,0:T(8,128)(2,1)S(1)} collective-permute-done((bf16[48,1024]{1,0:T(8,128)(2,1)S(1)}, bf16[48,1024]{1,0:T(8,128)(2,1)S(1)}, u32[]{:S(2)}, u32[]{:S(2)}) %collective-permute-start.24) | collective-permute-done | bytes 98336 | tf_op jit(solution)/shard_map/ppermute | solution.py:96
  183.3 1.1 slice_add_fusion.7
  184.5 3.3 %collective-permute-start.25 = (bf16[48,2048]{1,0:T(8,128)(2,1)S(1)}, bf16[48,2048]{1,0:T(8,128)(2,1)S(1)}, u32[]{:S(2)}, u32[]{:S(2)}) collective-permute-start(bf16[48,2048]{1,0:T(8,128)(2,1)S(1)} %pad_maximum_fusion.7), channel_id=1, source_target_pairs={{0,2},{2,4},{4,6},{6,8},{8,10},{10,12},{12,14},{14,0},{1,3},{3,5},... | collective-permute-start | bytes 589832 | tf_op jit(solution)/shard_map/ppermute | solution.py:96
  187.7 4.3 %collective-permute-done.28 = bf16[48,1024]{1,0:T(8,128)(2,1)S(1)} collective-permute-done((bf16[48,1024]{1,0:T(8,128)(2,1)S(1)}, bf16[48,1024]{1,0:T(8,128)(2,1)S(1)}, u32[]{:S(2)}, u32[]{:S(2)}) %collective-permute-start.28) | collective-permute-done | bytes 98336 | tf_op jit(solution)/shard_map/ppermute | solution.py:96
  192.1 0.9 slice_add_fusion.6
  193.1 3.3 %collective-permute-done.25 = bf16[48,2048]{1,0:T(8,128)(2,1)S(1)} collective-permute-done((bf16[48,2048]{1,0:T(8,128)(2,1)S(1)}, bf16[48,2048]{1,0:T(8,128)(2,1)S(1)}, u32[]{:S(2)}, u32[]{:S(2)}) %collective-permute-start.25) | collective-permute-done | bytes 196640 | tf_op jit(solution)/shard_map/ppermute | solution.py:96
  196.4 3.8 %collective-permute-start.26 = (bf16[48,2048]{1,0:T(8,128)(2,1)S(1)}, bf16[48,2048]{1,0:T(8,128)(2,1)S(1)}, u32[]{:S(2)}, u32[]{:S(2)}) collective-permute-start(bf16[48,2048]{1,0:T(8,128)(2,1)S(1)} %slice_add_fusion.2), channel_id=1, source_target_pairs={{0,2},{2,4},{4,6},{6,8},{8,10},{10,12},{12,14},{14,0},{1,3},{3,5},... | collective-permute-start | bytes 589832 | tf_op jit(solution)/shard_map/ppermute | solution.py:96
  200.2 4.4 %collective-permute-done.29 = bf16[48,2048]{1,0:T(8,128)(2,1)S(1)} collective-permute-done((bf16[48,2048]{1,0:T(8,128)(2,1)S(1)}, bf16[48,2048]{1,0:T(8,128)(2,1)S(1)}, u32[]{:S(2)}, u32[]{:S(2)}) %collective-permute-start.29) | collective-permute-done | bytes 196640 | tf_op jit(solution)/shard_map/ppermute | solution.py:96
  204.6 4.0 %collective-permute-done.26 = bf16[48,2048]{1,0:T(8,128)(2,1)S(1)} collective-permute-done((bf16[48,2048]{1,0:T(8,128)(2,1)S(1)}, bf16[48,2048]{1,0:T(8,128)(2,1)S(1)}, u32[]{:S(2)}, u32[]{:S(2)}) %collective-permute-start.26) | collective-permute-done | bytes 196640 | tf_op jit(solution)/shard_map/ppermute | solution.py:96
  208.7 3.8 %collective-permute-start.27 = (bf16[48,2048]{1,0:T(8,128)(2,1)S(1)}, bf16[48,2048]{1,0:T(8,128)(2,1)S(1)}, u32[]{:S(2)}, u32[]{:S(2)}) collective-permute-start(bf16[48,2048]{1,0:T(8,128)(2,1)S(1)} %get-tuple-element.25), channel_id=1, source_target_pairs={{0,2},{2,4},{4,6},{6,8},{8,10},{10,12},{12,14},{14,0},{1,3},{3,5},... | collective-permute-start | bytes 589832 | tf_op jit(solution)/shard_map/ppermute | solution.py:96
  212.5 8.2 %collective-permute-done.30 = bf16[48,2048]{1,0:T(8,128)(2,1)S(1)} collective-permute-done((bf16[48,2048]{1,0:T(8,128)(2,1)S(1)}, bf16[48,2048]{1,0:T(8,128)(2,1)S(1)}, u32[]{:S(2)}, u32[]{:S(2)}) %collective-permute-start.30) | collective-permute-done | bytes 196640 | tf_op jit(solution)/shard_map/ppermute | solution.py:96
  220.8 11.5 %collective-permute-done.31 = bf16[48,2048]{1,0:T(8,128)(2,1)S(1)} collective-permute-done((bf16[48,2048]{1,0:T(8,128)(2,1)S(1)}, bf16[48,2048]{1,0:T(8,128)(2,1)S(1)}, u32[]{:S(2)}, u32[]{:S(2)}) %collective-permute-start.31) | collective-permute-done | bytes 196640 | tf_op jit(solution)/shard_map/ppermute | solution.py:96
  232.4 0.8 reshape.167
  233.1 5.1 %all-to-all-start.2 = ((bf16[16,48,128]{2,1,0:T(8,128)(2,1)}), bf16[16,48,128]{2,1,0:T(8,128)(2,1)S(1)}, u32[]{:S(2)}, u32[]{:S(2)}) async-start(bf16[16,48,128]{2,1,0:T(8,128)(2,1)} %reshape.167), calls=%async_computation.4 | async-start | bytes 393216 | tf_op jit(solution)/shard_map/all_to_all | solution.py:316
  238.4 1.2 reshape.166
  239.6 7.0 %all-to-all-done.2 = bf16[16,48,128]{2,1,0:T(8,128)(2,1)S(1)} async-done(((bf16[16,48,128]{2,1,0:T(8,128)(2,1)}), bf16[16,48,128]{2,1,0:T(8,128)(2,1)S(1)}, u32[]{:S(2)}, u32[]{:S(2)}) %all-to-all-start.2) | async-done | bytes 196640 | tf_op jit(solution)/shard_map/all_to_all | solution.py:316
  246.6 12.7 %all_to_all.16 = bf16[16,112,128]{2,1,0:T(8,128)(2,1)S(1)} all-to-all(bf16[16,112,128]{2,1,0:T(8,128)(2,1)S(1)} %reshape.166), channel_id=1, replica_groups=mesh['sp'=16,'tp_0'=8,'tp_1'=2] {'sp'}, dimensions={0} | all-to-all | bytes 917504 | tf_op jit(solution)/shard_map/all_to_all | solution.py:316
  259.7 1.1 fusion.1
  (115 shorter events, 7.6 us)
Async XLA Ops:
  6.5 72.5 %reduce-scatter.3.cloned.1.call-start = ((), (), s32[]{:S(2)}) async-start(), calls=%async_computation.5 | async-start | bytes 2949120 | tf_op jit(solution)/shard_map/reduce_scatter | solution.py:300
  6.5 7.3 %copy-start.2 = (bf16[2048,128]{1,0:T(8,128)(2,1)S(1)}, bf16[2048,128]{1,0:T(8,128)(2,1)}, u32[]{:S(2)}) copy-start(bf16[2048,128]{1,0:T(8,128)(2,1)} %param.14) | copy-start | bytes 1572868
  6.5 7.9 %copy-start = (bf16[128,2048]{1,0:T(8,128)(2,1)S(1)}, bf16[128,2048]{1,0:T(8,128)(2,1)}, u32[]{:S(2)}) copy-start(bf16[128,2048]{1,0:T(8,128)(2,1)} %param.18) | copy-start | bytes 1572868
  7.9 8.9 %collective-permute-start.2 = (bf16[2,128,128]{2,1,0:T(8,128)(2,1)S(1)}, bf16[2,128,128]{2,1,0:T(8,128)(2,1)S(1)}, u32[]{:S(2)}, u32[]{:S(2)}) collective-permute-start(bf16[2,128,128]{2,1,0:T(8,128)(2,1)S(1)} %get-tuple-element.40), channel_id=1, source_target_pairs={{16,0},{32,16},{48,32},{64,48},{80,64},{96,80},{112,96},{128,112},... | collective-permute-start | bytes 196616 | tf_op jit(solution)/shard_map/ppermute | solution.py:33
  9.2 7.6 %collective-permute-start.1 = (bf16[2,128,128]{2,1,0:T(8,128)(2,1)S(1)}, bf16[2,128,128]{2,1,0:T(8,128)(2,1)S(1)}, u32[]{:S(2)}, u32[]{:S(2)}) collective-permute-start(bf16[2,128,128]{2,1,0:T(8,128)(2,1)S(1)} %get-tuple-element.39), channel_id=1, source_target_pairs={{0,16},{16,32},{32,48},{48,64},{64,80},{80,96},{96,112},{112,128},... | collective-permute-start | bytes 196616 | tf_op jit(solution)/shard_map/ppermute | solution.py:32
  13.9 3.6 %collective-permute-start = (bf16[8,1,128,128]{3,2,1,0:T(8,128)(2,1)S(1)}, bf16[8,1,128,128]{3,2,1,0:T(8,128)(2,1)S(1)}, u32[]{:S(2)}, u32[]{:S(2)}) collective-permute-start(bf16[8,1,128,128]{3,2,1,0:T(8,128)(2,1)S(1)} %get-tuple-element.42), channel_id=1, source_target_pairs={{0,1},{1,0},{2,3},{3,2},{4,5},{5,4},{6,7},{7,6},{8,9},{9,8},{10,11... | collective-permute-start | bytes 786440 | tf_op jit(solution)/shard_map/ppermute | solution.py:46
  14.0 2.1 collective-permute-start.3
  14.5 6.6 %collective-permute-start.4 = (bf16[128,2048]{1,0:T(8,128)(2,1)S(1)}, bf16[128,2048]{1,0:T(8,128)(2,1)S(1)}, u32[]{:S(2)}, u32[]{:S(2)}) collective-permute-start(bf16[128,2048]{1,0:T(8,128)(2,1)S(1)} %copy-done), channel_id=1, source_target_pairs={{0,1},{1,0},{2,3},{3,2},{4,5},{5,4},{6,7},{7,6},{8,9},{9,8},{10,11... | collective-permute-start | bytes 1572872 | tf_op jit(solution)/shard_map/ppermute | solution.py:290
  23.5 137.5 %all-gather.2.cloned.1.call-start = ((), (), s32[]{:S(2)}) async-start(), calls=%async_computation.6 | async-start | bytes 4386816 | tf_op jit(solution)/shard_map/all_gather | solution.py:330
  23.5 56.6 %collective-permute-start.13 = (bf16[3,2048,128]{2,1,0:T(8,128)(2,1)}, bf16[3,2048,128]{2,1,0:T(8,128)(2,1)}, u32[]{:S(2)}, u32[]{:S(2)}) collective-permute-start(bf16[3,2048,128]{2,1,0:T(8,128)(2,1)} %refs_0_.1), channel_id=1, source_target_pairs={{0,1},{1,0},{2,3},{3,2},{4,5},{5,4},{6,7},{7,6},{8,9},{9,8},{10,11... | collective-permute-start | bytes 4718600 | tf_op jit(solution)/shard_map/ppermute | solution.py:264
  24.0 56.1 %collective-permute-start.14 = (bf16[3,2048,128]{2,1,0:T(8,128)(2,1)}, bf16[3,2048,128]{2,1,0:T(8,128)(2,1)}, u32[]{:S(2)}, u32[]{:S(2)}) collective-permute-start(bf16[3,2048,128]{2,1,0:T(8,128)(2,1)} %refs_2_.1), channel_id=1, source_target_pairs={{0,1},{1,0},{2,3},{3,2},{4,5},{5,4},{6,7},{7,6},{8,9},{9,8},{10,11... | collective-permute-start | bytes 4718600 | tf_op jit(solution)/shard_map/ppermute | solution.py:264
  24.1 56.0 %collective-permute-start.15 = (bf16[3,128,2048]{2,1,0:T(8,128)(2,1)}, bf16[3,128,2048]{2,1,0:T(8,128)(2,1)}, u32[]{:S(2)}, u32[]{:S(2)}) collective-permute-start(bf16[3,128,2048]{2,1,0:T(8,128)(2,1)} %refs_4_.1), channel_id=1, source_target_pairs={{0,1},{1,0},{2,3},{3,2},{4,5},{5,4},{6,7},{7,6},{8,9},{9,8},{10,11... | collective-permute-start | bytes 4718600 | tf_op jit(solution)/shard_map/ppermute | solution.py:264
  24.5 3.9 %copy-start.6 = (s32[128]{0:T(128)S(1)}, s32[128]{0:T(128)}, u32[]{:S(2)}) copy-start(s32[128]{0:T(128)} %param.22) | copy-start | bytes 1540
  24.5 4.0 %copy-start.8 = (bf16[128,2]{0,1:T(2,128)(2,1)S(1)}, bf16[128,2]{0,1:T(2,128)(2,1)}, u32[]{:S(2)}) copy-start(bf16[128,2]{0,1:T(2,128)(2,1)} %param.24) | copy-start | bytes 1540
  25.2 16.8 %copy-start.7 = (s32[128,2]{0,1:T(2,128)S(1)}, s32[128,2]{0,1:T(2,128)}, u32[]{:S(2)}) copy-start(s32[128,2]{0,1:T(2,128)} %param.23) | copy-start | bytes 3076
  25.2 5.5 %collective-permute-start.5 = (bf16[128,384]{1,0:T(8,128)(2,1)S(1)}, bf16[128,384]{1,0:T(8,128)(2,1)S(1)}, u32[]{:S(2)}, u32[]{:S(2)}) collective-permute-start(bf16[128,384]{1,0:T(8,128)(2,1)S(1)} %get-tuple-element.47), channel_id=1, source_target_pairs={{0,2},{2,4},{4,6},{6,8},{8,10},{10,12},{12,14},{14,0},{1,3},{3,5},... | collective-permute-start | bytes 294920 | tf_op jit(solution)/shard_map/ppermute | solution.py:96
  28.5 6.0 %collective-permute-start.9 = (bf16[128,384]{1,0:T(8,128)(2,1)S(1)}, bf16[128,384]{1,0:T(8,128)(2,1)S(1)}, u32[]{:S(2)}, u32[]{:S(2)}) collective-permute-start(bf16[128,384]{1,0:T(8,128)(2,1)S(1)} %get-tuple-element.48), channel_id=1, source_target_pairs={{0,14},{2,0},{4,2},{6,4},{8,6},{10,8},{12,10},{14,12},{1,15},{3,1}... | collective-permute-start | bytes 294920 | tf_op jit(solution)/shard_map/ppermute | solution.py:96
  30.8 7.4 %collective-permute-start.6 = (bf16[128,768]{1,0:T(8,128)(2,1)S(1)}, bf16[128,768]{1,0:T(8,128)(2,1)S(1)}, u32[]{:S(2)}, u32[]{:S(2)}) collective-permute-start(bf16[128,768]{1,0:T(8,128)(2,1)S(1)} %pad_maximum_fusion.5), channel_id=1, source_target_pairs={{0,2},{2,4},{4,6},{6,8},{8,10},{10,12},{12,14},{14,0},{1,3},{3,5},... | collective-permute-start | bytes 589832 | tf_op jit(solution)/shard_map/ppermute | solution.py:96
  34.6 7.8 %collective-permute-start.10 = (bf16[128,768]{1,0:T(8,128)(2,1)S(1)}, bf16[128,768]{1,0:T(8,128)(2,1)S(1)}, u32[]{:S(2)}, u32[]{:S(2)}) collective-permute-start(bf16[128,768]{1,0:T(8,128)(2,1)S(1)} %pad_maximum_fusion.6), channel_id=1, source_target_pairs={{0,14},{2,0},{4,2},{6,4},{8,6},{10,8},{12,10},{14,12},{1,15},{3,1}... | collective-permute-start | bytes 589832 | tf_op jit(solution)/shard_map/ppermute | solution.py:96
  38.2 11.6 %collective-permute-start.7 = (bf16[128,768]{1,0:T(8,128)(2,1)S(1)}, bf16[128,768]{1,0:T(8,128)(2,1)S(1)}, u32[]{:S(2)}, u32[]{:S(2)}) collective-permute-start(bf16[128,768]{1,0:T(8,128)(2,1)S(1)} %bitcast_add_fusion.2), channel_id=1, source_target_pairs={{0,2},{2,4},{4,6},{6,8},{8,10},{10,12},{12,14},{14,0},{1,3},{3,5},... | collective-permute-start | bytes 589832 | tf_op jit(solution)/shard_map/ppermute | solution.py:96
  49.8 12.3 %collective-permute-start.11 = (bf16[128,768]{1,0:T(8,128)(2,1)S(1)}, bf16[128,768]{1,0:T(8,128)(2,1)S(1)}, u32[]{:S(2)}, u32[]{:S(2)}) collective-permute-start(bf16[128,768]{1,0:T(8,128)(2,1)S(1)} %get-tuple-element.32), channel_id=1, source_target_pairs={{0,14},{2,0},{4,2},{6,4},{8,6},{10,8},{12,10},{14,12},{1,15},{3,1}... | collective-permute-start | bytes 589832 | tf_op jit(solution)/shard_map/ppermute | solution.py:96
  49.9 12.6 %collective-permute-start.8 = (bf16[128,768]{1,0:T(8,128)(2,1)S(1)}, bf16[128,768]{1,0:T(8,128)(2,1)S(1)}, u32[]{:S(2)}, u32[]{:S(2)}) collective-permute-start(bf16[128,768]{1,0:T(8,128)(2,1)S(1)} %get-tuple-element.31), channel_id=1, source_target_pairs={{0,2},{2,4},{4,6},{6,8},{8,10},{10,12},{12,14},{14,0},{1,3},{3,5},... | collective-permute-start | bytes 589832 | tf_op jit(solution)/shard_map/ppermute | solution.py:96
  62.2 11.6 %collective-permute-start.12 = (bf16[128,768]{1,0:T(8,128)(2,1)S(1)}, bf16[128,768]{1,0:T(8,128)(2,1)S(1)}, u32[]{:S(2)}, u32[]{:S(2)}) collective-permute-start(bf16[128,768]{1,0:T(8,128)(2,1)S(1)} %bitcast_add_fusion.1), channel_id=1, source_target_pairs={{0,14},{2,0},{4,2},{6,4},{8,6},{10,8},{12,10},{14,12},{1,15},{3,1}... | collective-permute-start | bytes 589832 | tf_op jit(solution)/shard_map/ppermute | solution.py:96
  62.5 17.9 %copy-start.3 = (bf16[128,2048]{1,0:T(8,128)(2,1)S(1)}, bf16[128,2048]{1,0:T(8,128)(2,1)}, u32[]{:S(2)}) copy-start(bf16[128,2048]{1,0:T(8,128)(2,1)} %param.19) | copy-start | bytes 1572868
  62.5 17.8 %copy-start.4 = (f32[2048]{0:T(1024)S(1)}, f32[2048]{0:T(1024)}, u32[]{:S(2)}) copy-start(f32[2048]{0:T(1024)} %param.20) | copy-start | bytes 24580
  80.1 0.7 copy-start.5
  102.1 136.3 %reduce-scatter.5.cloned.1.call-start = ((), (), s32[]{:S(2)}) async-start(), calls=%async_computation.7 | async-start | bytes 4128768 | tf_op jit(solution)/shard_map/reduce_scatter | solution.py:335
  103.6 6.8 %collective-permute-start.16 = (bf16[48,2176]{1,0:T(8,128)(2,1)S(1)}, bf16[48,2176]{1,0:T(8,128)(2,1)S(1)}, u32[]{:S(2)}, u32[]{:S(2)}) collective-permute-start(bf16[48,2176]{1,0:T(8,128)(2,1)S(1)} %get-tuple-element.51), channel_id=1, source_target_pairs={{0,2},{2,4},{4,6},{6,8},{8,10},{10,12},{12,14},{14,0},{1,3},{3,5},... | collective-permute-start | bytes 626696 | tf_op jit(solution)/shard_map/ppermute | solution.py:96
  105.1 7.0 %collective-permute-start.17 = (bf16[48,2176]{1,0:T(8,128)(2,1)S(1)}, bf16[48,2176]{1,0:T(8,128)(2,1)S(1)}, u32[]{:S(2)}, u32[]{:S(2)}) collective-permute-start(bf16[48,2176]{1,0:T(8,128)(2,1)S(1)} %get-tuple-element.51), channel_id=1, source_target_pairs={{0,14},{2,0},{4,2},{6,4},{8,6},{10,8},{12,10},{14,12},{1,15},{3,1}... | collective-permute-start | bytes 626696 | tf_op jit(solution)/shard_map/ppermute | solution.py:96
  110.4 11.4 %collective-permute-start.18 = (bf16[48,2176]{1,0:T(8,128)(2,1)S(1)}, bf16[48,2176]{1,0:T(8,128)(2,1)S(1)}, u32[]{:S(2)}, u32[]{:S(2)}) collective-permute-start(bf16[48,2176]{1,0:T(8,128)(2,1)S(1)} %collective-permute-done.16), channel_id=1, source_target_pairs={{0,2},{2,4},{4,6},{6,8},{8,10},{10,12},{12,14},{14,0},{1,3},{3,5},... | collective-permute-start | bytes 626696 | tf_op jit(solution)/shard_map/ppermute | solution.py:96
  112.1 12.4 %collective-permute-start.19 = (bf16[48,2176]{1,0:T(8,128)(2,1)S(1)}, bf16[48,2176]{1,0:T(8,128)(2,1)S(1)}, u32[]{:S(2)}, u32[]{:S(2)}) collective-permute-start(bf16[48,2176]{1,0:T(8,128)(2,1)S(1)} %collective-permute-done.17), channel_id=1, source_target_pairs={{0,14},{2,0},{4,2},{6,4},{8,6},{10,8},{12,10},{14,12},{1,15},{3,1}... | collective-permute-start | bytes 626696 | tf_op jit(solution)/shard_map/ppermute | solution.py:96
  121.8 15.1 %collective-permute-start.20 = (bf16[48,2176]{1,0:T(8,128)(2,1)S(1)}, bf16[48,2176]{1,0:T(8,128)(2,1)S(1)}, u32[]{:S(2)}, u32[]{:S(2)}) collective-permute-start(bf16[48,2176]{1,0:T(8,128)(2,1)S(1)} %collective-permute-done.18), channel_id=1, source_target_pairs={{0,2},{2,4},{4,6},{6,8},{8,10},{10,12},{12,14},{14,0},{1,3},{3,5},... | collective-permute-start | bytes 626696 | tf_op jit(solution)/shard_map/ppermute | solution.py:96
  124.5 12.3 %collective-permute-start.21 = (bf16[48,2176]{1,0:T(8,128)(2,1)S(1)}, bf16[48,2176]{1,0:T(8,128)(2,1)S(1)}, u32[]{:S(2)}, u32[]{:S(2)}) collective-permute-start(bf16[48,2176]{1,0:T(8,128)(2,1)S(1)} %collective-permute-done.19), channel_id=1, source_target_pairs={{0,14},{2,0},{4,2},{6,4},{8,6},{10,8},{12,10},{14,12},{1,15},{3,1}... | collective-permute-start | bytes 626696 | tf_op jit(solution)/shard_map/ppermute | solution.py:96
  136.8 8.5 %collective-permute-start.23 = (bf16[48,1152]{1,0:T(8,128)(2,1)S(1)}, bf16[48,1152]{1,0:T(8,128)(2,1)S(1)}, u32[]{:S(2)}, u32[]{:S(2)}) collective-permute-start(bf16[48,1152]{1,0:T(8,128)(2,1)S(1)} %slice.152), channel_id=1, source_target_pairs={{0,14},{2,0},{4,2},{6,4},{8,6},{10,8},{12,10},{14,12},{1,15},{3,1}... | collective-permute-start | bytes 331784 | tf_op jit(solution)/shard_map/ppermute | solution.py:96
  137.0 7.9 %collective-permute-start.22 = (bf16[48,1024]{1,0:T(8,128)(2,1)S(1)}, bf16[48,1024]{1,0:T(8,128)(2,1)S(1)}, u32[]{:S(2)}, u32[]{:S(2)}) collective-permute-start(bf16[48,1024]{1,0:T(8,128)(2,1)S(1)} %slice.151), channel_id=1, source_target_pairs={{0,2},{2,4},{4,6},{6,8},{8,10},{10,12},{12,14},{14,0},{1,3},{3,5},... | collective-permute-start | bytes 294920 | tf_op jit(solution)/shard_map/ppermute | solution.py:96
  177.6 18.7 %copy-start.1 = (bf16[384,2048]{1,0:T(8,128)(2,1)S(1)}, bf16[384,2048]{1,0:T(8,128)(2,1)}, u32[]{:S(2)}) copy-start(bf16[384,2048]{1,0:T(8,128)(2,1)} %experts.2) | copy-start | bytes 4718596
  178.7 4.6 %collective-permute-start.24 = (bf16[48,1024]{1,0:T(8,128)(2,1)S(1)}, bf16[48,1024]{1,0:T(8,128)(2,1)S(1)}, u32[]{:S(2)}, u32[]{:S(2)}) collective-permute-start(bf16[48,1024]{1,0:T(8,128)(2,1)S(1)} %slice.130), channel_id=1, source_target_pairs={{0,2},{2,4},{4,6},{6,8},{8,10},{10,12},{12,14},{14,0},{1,3},{3,5},... | collective-permute-start | bytes 294920 | tf_op jit(solution)/shard_map/ppermute | solution.py:96
  184.3 7.7 %collective-permute-start.28 = (bf16[48,1024]{1,0:T(8,128)(2,1)S(1)}, bf16[48,1024]{1,0:T(8,128)(2,1)S(1)}, u32[]{:S(2)}, u32[]{:S(2)}) collective-permute-start(bf16[48,1024]{1,0:T(8,128)(2,1)S(1)} %get-tuple-element.28), channel_id=1, source_target_pairs={{0,14},{2,0},{4,2},{6,4},{8,6},{10,8},{12,10},{14,12},{1,15},{3,1}... | collective-permute-start | bytes 294920 | tf_op jit(solution)/shard_map/ppermute | solution.py:96
  184.5 11.9 %collective-permute-start.25 = (bf16[48,2048]{1,0:T(8,128)(2,1)S(1)}, bf16[48,2048]{1,0:T(8,128)(2,1)S(1)}, u32[]{:S(2)}, u32[]{:S(2)}) collective-permute-start(bf16[48,2048]{1,0:T(8,128)(2,1)S(1)} %pad_maximum_fusion.7), channel_id=1, source_target_pairs={{0,2},{2,4},{4,6},{6,8},{8,10},{10,12},{12,14},{14,0},{1,3},{3,5},... | collective-permute-start | bytes 589832 | tf_op jit(solution)/shard_map/ppermute | solution.py:96
  193.0 11.6 %collective-permute-start.29 = (bf16[48,2048]{1,0:T(8,128)(2,1)S(1)}, bf16[48,2048]{1,0:T(8,128)(2,1)S(1)}, u32[]{:S(2)}, u32[]{:S(2)}) collective-permute-start(bf16[48,2048]{1,0:T(8,128)(2,1)S(1)} %pad_maximum_fusion.8), channel_id=1, source_target_pairs={{0,14},{2,0},{4,2},{6,4},{8,6},{10,8},{12,10},{14,12},{1,15},{3,1}... | collective-permute-start | bytes 589832 | tf_op jit(solution)/shard_map/ppermute | solution.py:96
  196.4 12.2 %collective-permute-start.26 = (bf16[48,2048]{1,0:T(8,128)(2,1)S(1)}, bf16[48,2048]{1,0:T(8,128)(2,1)S(1)}, u32[]{:S(2)}, u32[]{:S(2)}) collective-permute-start(bf16[48,2048]{1,0:T(8,128)(2,1)S(1)} %slice_add_fusion.2), channel_id=1, source_target_pairs={{0,2},{2,4},{4,6},{6,8},{8,10},{10,12},{12,14},{14,0},{1,3},{3,5},... | collective-permute-start | bytes 589832 | tf_op jit(solution)/shard_map/ppermute | solution.py:96
  208.6 12.1 %collective-permute-start.30 = (bf16[48,2048]{1,0:T(8,128)(2,1)S(1)}, bf16[48,2048]{1,0:T(8,128)(2,1)S(1)}, u32[]{:S(2)}, u32[]{:S(2)}) collective-permute-start(bf16[48,2048]{1,0:T(8,128)(2,1)S(1)} %get-tuple-element.26), channel_id=1, source_target_pairs={{0,14},{2,0},{4,2},{6,4},{8,6},{10,8},{12,10},{14,12},{1,15},{3,1}... | collective-permute-start | bytes 589832 | tf_op jit(solution)/shard_map/ppermute | solution.py:96
  208.7 12.1 %collective-permute-start.27 = (bf16[48,2048]{1,0:T(8,128)(2,1)S(1)}, bf16[48,2048]{1,0:T(8,128)(2,1)S(1)}, u32[]{:S(2)}, u32[]{:S(2)}) collective-permute-start(bf16[48,2048]{1,0:T(8,128)(2,1)S(1)} %get-tuple-element.25), channel_id=1, source_target_pairs={{0,2},{2,4},{4,6},{6,8},{8,10},{10,12},{12,14},{14,0},{1,3},{3,5},... | collective-permute-start | bytes 589832 | tf_op jit(solution)/shard_map/ppermute | solution.py:96
  220.7 11.6 %collective-permute-start.31 = (bf16[48,2048]{1,0:T(8,128)(2,1)S(1)}, bf16[48,2048]{1,0:T(8,128)(2,1)S(1)}, u32[]{:S(2)}, u32[]{:S(2)}) collective-permute-start(bf16[48,2048]{1,0:T(8,128)(2,1)S(1)} %slice_add_fusion.1), channel_id=1, source_target_pairs={{0,14},{2,0},{4,2},{6,4},{8,6},{10,8},{12,10},{14,12},{1,15},{3,1}... | collective-permute-start | bytes 589832 | tf_op jit(solution)/shard_map/ppermute | solution.py:96
  233.1 13.5 %all-to-all-start.2 = ((bf16[16,48,128]{2,1,0:T(8,128)(2,1)}), bf16[16,48,128]{2,1,0:T(8,128)(2,1)S(1)}, u32[]{:S(2)}, u32[]{:S(2)}) async-start(bf16[16,48,128]{2,1,0:T(8,128)(2,1)} %reshape.167), calls=%async_computation.4 | async-start | bytes 393216 | tf_op jit(solution)/shard_map/all_to_all | solution.py:316
Sparse Core Ops, SparseCore 0:
  23.6 55.3 reduce-scatter.2
  102.2 58.7 all-gather.1
  177.7 60.6 reduce-scatter.4
where the time goes:
time: 268 us; the launch traced here: 267 us
  waiting for transfers between devices  117 us (44%)
  starting transfers between devices  49.3 us (18%)
  blocking collectives  32.1 us (12%)
  Pallas kernels  27.1 us (10%)
  between operations  14.5 us (5%)
  local copies, waits for them, and re-layouts  11.6 us (4%)
  other arithmetic  9.21 us (3%)
  matrix products  6.81 us (3%)
    ppermute x12, waiting for transfers between devices, shifts(): lax.ppermute(a, Z, down)  59.7 us
    ppermute x12, waiting for transfers between devices, shifts(): lax.ppermute(a, Z, up)  40.2 us
    ppermute x12, starting transfers between devices, shifts(): lax.ppermute(a, Z, up)  34.7 us
    all_to_all x2, blocking collectives, exchange(): lax.all_to_all(rows.reshape(groups, -1, LANES), 'sp', split_axis=0, conca...  32.1 us
    pallas_call x2, Pallas kernels, experts(): pl.pallas_call(experts_kernel, in_specs=[anywhere] * 7, out_specs=anywher...  27.1 us
    all_to_all x1, waiting for transfers between devices, exchange(): lax.all_to_all(rows.reshape(groups, -1, LANES), 'sp', split_axis=0, conca...  6.96 us
  transfers between devices with their start and end apart: 36, of which 21 were waited for; matrix products, arithmetic and copies ran while one was open for 7% of the time, Pallas kernels for 4%

commit v1 on v0

--- a/solution.py
+++ b/solution.py
@@ -137,7 +137,8 @@
     wide = 512
 
     def span(i):
-        return pl.ds(pl.multiple_of(i * step, 16), step)
+        start = i * step
+        return pl.ds(start if isinstance(i, int) else pl.multiple_of(start, 16), step)
 
     def weight_copy(k, e):
         return pltpu.make_async_copy(weights_in[k].at[e], weights[k].at[e], weight_sems.at[k, e])
@@ -164,10 +165,9 @@
         for k in range(4):
             weight_copy(k, e).wait()
 
-        @pl.loop(0, steps)
-        def _(i):
+        for i in range(steps):
             @pl.when(e == 0)
-            def _():
+            def _(i=i):
                 row_copy(i).wait()
 
             joined = jnp.concatenate([gate_own[e], gate_far[e], up_own[e], up_far[e]], axis=1)

time: 268 us -> 268 us (level)
  no operation moved by 1% of the time
where the time goes in v1:
time: 268 us; the launch traced here: 267 us
  waiting for transfers between devices  117 us (44%)
  starting transfers between devices  49.3 us (18%)
  blocking collectives  32.1 us (12%)
  Pallas kernels  27.1 us (10%)
  between operations  14.5 us (5%)
  local copies, waits for them, and re-layouts  11.6 us (4%)
  other arithmetic  9.21 us (3%)
  matrix products  6.81 us (3%)
    ppermute x12, waiting for transfers between devices, shifts(): lax.ppermute(a, Z, down)  59.7 us
    ppermute x12, waiting for transfers between devices, shifts(): lax.ppermute(a, Z, up)  40.2 us
    ppermute x12, starting transfers between devices, shifts(): lax.ppermute(a, Z, up)  34.7 us
    all_to_all x2, blocking collectives, exchange(): lax.all_to_all(rows.reshape(groups, -1, LANES), 'sp', split_axis=0, conca...  32.1 us
    pallas_call x2, Pallas kernels, experts(): pl.pallas_call(experts_kernel, in_specs=[anywhere] * 7, out_specs=anywher...  27.1 us
    all_to_all x1, waiting for transfers between devices, exchange(): lax.all_to_all(rows.reshape(groups, -1, LANES), 'sp', split_axis=0, conca...  6.96 us
  transfers between devices with their start and end apart: 36, of which 21 were waited for; matrix products, arithmetic and copies ran while one was open for 7% of the time, Pallas kernels for 4%

profile of v1, /device:TPU:96, one launch (start us, length us, event | category | flops | bytes accessed | tf_op | source)
XLA Modules:
  0.0 267.3 jit_solution(14747559045985611009)
XLA Ops:
  6.5 1.4 dynamic-slice_bitcast_fusion
  7.9 1.3 collective-permute-start.2
  9.2 4.5 %collective-permute-start.1 = (bf16[2,128,128]{2,1,0:T(8,128)(2,1)S(1)}, bf16[2,128,128]{2,1,0:T(8,128)(2,1)S(1)}, u32[]{:S(2)}, u32[]{:S(2)}) collective-permute-start(bf16[2,128,128]{2,1,0:T(8,128)(2,1)S(1)} %get-tuple-element.39), channel_id=1, source_target_pairs={{0,16},{16,32},{32,48},{48,64},{64,80},{80,96},{96,112},{112,128},... | collective-permute-start | bytes 196616 | tf_op jit(solution)/shard_map/ppermute | solution.py:32
  15.4 0.6 fusion.4
  16.1 0.7 pad_maximum_fusion.11
  17.4 0.9 fusion
  18.4 1.3 fusion.2
  19.7 1.3 fusion.7
  21.1 2.3 bitcast_convert_fusion
  24.5 0.6 bitcast_convert_fusion.1
  25.2 3.2 %collective-permute-start.5 = (bf16[128,384]{1,0:T(8,128)(2,1)S(1)}, bf16[128,384]{1,0:T(8,128)(2,1)S(1)}, u32[]{:S(2)}, u32[]{:S(2)}) collective-permute-start(bf16[128,384]{1,0:T(8,128)(2,1)S(1)} %get-tuple-element.47), channel_id=1, source_target_pairs={{0,2},{2,4},{4,6},{6,8},{8,10},{10,12},{12,14},{14,0},{1,3},{3,5},... | collective-permute-start | bytes 294920 | tf_op jit(solution)/shard_map/ppermute | solution.py:96
  28.6 2.1 collective-permute-done.5
  30.8 3.8 %collective-permute-start.6 = (bf16[128,768]{1,0:T(8,128)(2,1)S(1)}, bf16[128,768]{1,0:T(8,128)(2,1)S(1)}, u32[]{:S(2)}, u32[]{:S(2)}) collective-permute-start(bf16[128,768]{1,0:T(8,128)(2,1)S(1)} %pad_maximum_fusion.5), channel_id=1, source_target_pairs={{0,2},{2,4},{4,6},{6,8},{8,10},{10,12},{12,14},{14,0},{1,3},{3,5},... | collective-permute-start | bytes 589832 | tf_op jit(solution)/shard_map/ppermute | solution.py:96
  34.9 3.3 %collective-permute-done.6 = bf16[128,768]{1,0:T(8,128)(2,1)S(1)} collective-permute-done((bf16[128,768]{1,0:T(8,128)(2,1)S(1)}, bf16[128,768]{1,0:T(8,128)(2,1)S(1)}, u32[]{:S(2)}, u32[]{:S(2)}) %collective-permute-start.6) | collective-permute-done | bytes 196640 | tf_op jit(solution)/shard_map/ppermute | solution.py:96
  38.2 3.8 %collective-permute-start.7 = (bf16[128,768]{1,0:T(8,128)(2,1)S(1)}, bf16[128,768]{1,0:T(8,128)(2,1)S(1)}, u32[]{:S(2)}, u32[]{:S(2)}) collective-permute-start(bf16[128,768]{1,0:T(8,128)(2,1)S(1)} %bitcast_add_fusion.2), channel_id=1, source_target_pairs={{0,2},{2,4},{4,6},{6,8},{8,10},{10,12},{12,14},{14,0},{1,3},{3,5},... | collective-permute-start | bytes 589832 | tf_op jit(solution)/shard_map/ppermute | solution.py:96
  42.4 7.4 %collective-permute-done.7 = bf16[128,768]{1,0:T(8,128)(2,1)S(1)} collective-permute-done((bf16[128,768]{1,0:T(8,128)(2,1)S(1)}, bf16[128,768]{1,0:T(8,128)(2,1)S(1)}, u32[]{:S(2)}, u32[]{:S(2)}) %collective-permute-start.7) | collective-permute-done | bytes 196640 | tf_op jit(solution)/shard_map/ppermute | solution.py:96
  49.9 3.8 %collective-permute-start.8 = (bf16[128,768]{1,0:T(8,128)(2,1)S(1)}, bf16[128,768]{1,0:T(8,128)(2,1)S(1)}, u32[]{:S(2)}, u32[]{:S(2)}) collective-permute-start(bf16[128,768]{1,0:T(8,128)(2,1)S(1)} %get-tuple-element.31), channel_id=1, source_target_pairs={{0,2},{2,4},{4,6},{6,8},{8,10},{10,12},{12,14},{14,0},{1,3},{3,5},... | collective-permute-start | bytes 589832 | tf_op jit(solution)/shard_map/ppermute | solution.py:96
  53.7 8.5 %collective-permute-done.11 = bf16[128,768]{1,0:T(8,128)(2,1)S(1)} collective-permute-done((bf16[128,768]{1,0:T(8,128)(2,1)S(1)}, bf16[128,768]{1,0:T(8,128)(2,1)S(1)}, u32[]{:S(2)}, u32[]{:S(2)}) %collective-permute-start.11) | collective-permute-done | bytes 196640 | tf_op jit(solution)/shard_map/ppermute | solution.py:96
  62.5 11.3 %collective-permute-done.12 = bf16[128,768]{1,0:T(8,128)(2,1)S(1)} collective-permute-done((bf16[128,768]{1,0:T(8,128)(2,1)S(1)}, bf16[128,768]{1,0:T(8,128)(2,1)S(1)}, u32[]{:S(2)}, u32[]{:S(2)}) %collective-permute-start.12) | collective-permute-done | bytes 196640 | tf_op jit(solution)/shard_map/ppermute | solution.py:96
  73.8 5.2 %reduce-scatter.3.cloned.1.call-done = bf16[128,1280]{1,0:T(8,128)(2,1)} async-done(((bf16[1024,1280]{1,0:T(8,128)(2,1)}), bf16[128,1280]{1,0:T(8,128)(2,1)}) %reduce-scatter.3.cloned.1.call-update) | async-done | bytes 327696 | tf_op jit(solution)/shard_map/reduce_scatter | solution.py:300
  79.0 1.1 maximum_convert_fusion
  81.6 19.4 %all_to_all.15 = bf16[16,176,128]{2,1,0:T(8,128)(2,1)S(1)} all-to-all(bf16[16,176,128]{2,1,0:T(8,128)(2,1)S(1)} %fusion.12), channel_id=1, replica_groups=mesh['sp'=16,'tp_0'=8,'tp_1'=2] {'sp'}, dimensions={0} | all-to-all | bytes 1441792 | tf_op jit(solution)/shard_map/all_to_all | solution.py:316
  101.2 0.8 pad_maximum_fusion.3
  102.3 0.7 constant_dynamic-update-slice_fusion.1
  103.0 0.6 constant_dynamic-update-slice_fusion
  103.6 1.4 collective-permute-start.16
  105.1 0.6 collective-permute-start.17
  105.7 4.7 %collective-permute-done.16 = bf16[48,2176]{1,0:T(8,128)(2,1)S(1)} collective-permute-done((bf16[48,2176]{1,0:T(8,128)(2,1)S(1)}, bf16[48,2176]{1,0:T(8,128)(2,1)S(1)}, u32[]{:S(2)}, u32[]{:S(2)}) %collective-permute-start.16) | collective-permute-done | bytes 208928 | tf_op jit(solution)/shard_map/ppermute | solution.py:96
  110.4 1.7 collective-permute-start.18
  112.4 0.7 constant_dynamic-update-slice_fusion.7
  113.1 0.7 constant_dynamic-update-slice_fusion.6
  113.9 8.0 %collective-permute-done.18 = bf16[48,2176]{1,0:T(8,128)(2,1)S(1)} collective-permute-done((bf16[48,2176]{1,0:T(8,128)(2,1)S(1)}, bf16[48,2176]{1,0:T(8,128)(2,1)S(1)}, u32[]{:S(2)}, u32[]{:S(2)}) %collective-permute-start.18) | collective-permute-done | bytes 208928 | tf_op jit(solution)/shard_map/ppermute | solution.py:96
  121.8 2.7 collective-permute-start.20
  124.5 0.7 constant_dynamic-update-slice_fusion.5
  125.2 0.7 constant_dynamic-update-slice_fusion.4
  125.9 10.9 %collective-permute-done.21 = bf16[48,2176]{1,0:T(8,128)(2,1)S(1)} collective-permute-done((bf16[48,2176]{1,0:T(8,128)(2,1)S(1)}, bf16[48,2176]{1,0:T(8,128)(2,1)S(1)}, u32[]{:S(2)}, u32[]{:S(2)}) %collective-permute-start.21) | collective-permute-done | bytes 208928 | tf_op jit(solution)/shard_map/ppermute | solution.py:96
  137.0 3.5 %collective-permute-start.22 = (bf16[48,1024]{1,0:T(8,128)(2,1)S(1)}, bf16[48,1024]{1,0:T(8,128)(2,1)S(1)}, u32[]{:S(2)}, u32[]{:S(2)}) collective-permute-start(bf16[48,1024]{1,0:T(8,128)(2,1)S(1)} %slice.151), channel_id=1, source_target_pairs={{0,2},{2,4},{4,6},{6,8},{8,10},{10,12},{12,14},{14,0},{1,3},{3,5},... | collective-permute-start | bytes 294920 | tf_op jit(solution)/shard_map/ppermute | solution.py:96
  140.5 0.7 constant_dynamic-update-slice_fusion.3
  141.2 0.7 constant_dynamic-update-slice_fusion.2
  141.9 3.0 %collective-permute-done.22 = bf16[48,1024]{1,0:T(8,128)(2,1)S(1)} collective-permute-done((bf16[48,1024]{1,0:T(8,128)(2,1)S(1)}, bf16[48,1024]{1,0:T(8,128)(2,1)S(1)}, u32[]{:S(2)}, u32[]{:S(2)}) %collective-permute-start.22) | collective-permute-done | bytes 98336 | tf_op jit(solution)/shard_map/ppermute | solution.py:96
  144.8 0.5 collective-permute-done.23
  145.4 0.7 maximum_dynamic-update-slice_fusion.rows_in
  146.1 10.5 %experts.2 = bf16[384,2048]{1,0:T(8,128)(2,1)} custom-call(bf16[384,2176]{1,0:T(8,128)(2,1)} %maximum_dynamic-update-slice_fusion.rows_in, bf16[3,2048,128]{2,1,0:T(8,128)(2,1)} %refs_0_.1, bf16[3,2048,128]{2,1,0:T(8,128)(2,1)} %collective-permute-done.13.refs_1_, bf16[3,2048,128]{2,1,0:T(8,128)(2,1)} %refs_2_.1, ...), custom_call_target="tpu_custom_call" | custom-call | flops 3623878656 | bytes 20971520 | tf_op jit(solution)/shard_map/experts/pallas_call | solution.py:215
  156.6 4.4 %all-gather.2.cloned.1.call-done.rows_in = bf16[896,2176]{1,0:T(8,128)(2,1)} async-done(((bf16[112,2176]{1,0:T(8,128)(2,1)}), bf16[896,2176]{1,0:T(8,128)(2,1)}) %all-gather.2.cloned.1.call-update) | async-done | bytes 3899408 | tf_op jit(solution)/shard_map/all_gather | solution.py:330
  161.0 16.6 %experts.3 = bf16[896,2048]{1,0:T(8,128)(2,1)} custom-call(bf16[896,2176]{1,0:T(8,128)(2,1)} %all-gather.2.cloned.1.call-done.rows_in, bf16[3,2048,128]{2,1,0:T(8,128)(2,1)} %refs_0_.1, bf16[3,2048,128]{2,1,0:T(8,128)(2,1)} %collective-permute-done.13.refs_1_, bf16[3,2048,128]{2,1,0:T(8,128)(2,1)} %refs_2_.1, ...), custom_call_target="tpu_custom_call" | custom-call | flops 8455716864 | bytes 20971520 | tf_op jit(solution)/shard_map/experts/pallas_call | solution.py:215
  177.6 1.0 slice.130
  178.7 4.6 %collective-permute-done.24 = bf16[48,1024]{1,0:T(8,128)(2,1)S(1)} collective-permute-done((bf16[48,1024]{1,0:T(8,128)(2,1)S(1)}, bf16[48,1024]{1,0:T(8,128)(2,1)S(1)}, u32[]{:S(2)}, u32[]{:S(2)}) %collective-permute-start.24) | collective-permute-done | bytes 98336 | tf_op jit(solution)/shard_map/ppermute | solution.py:96
  183.3 1.1 slice_add_fusion.7
  184.5 3.3 %collective-permute-start.25 = (bf16[48,2048]{1,0:T(8,128)(2,1)S(1)}, bf16[48,2048]{1,0:T(8,128)(2,1)S(1)}, u32[]{:S(2)}, u32[]{:S(2)}) collective-permute-start(bf16[48,2048]{1,0:T(8,128)(2,1)S(1)} %pad_maximum_fusion.7), channel_id=1, source_target_pairs={{0,2},{2,4},{4,6},{6,8},{8,10},{10,12},{12,14},{14,0},{1,3},{3,5},... | collective-permute-start | bytes 589832 | tf_op jit(solution)/shard_map/ppermute | solution.py:96
  187.7 4.3 %collective-permute-done.28 = bf16[48,1024]{1,0:T(8,128)(2,1)S(1)} collective-permute-done((bf16[48,1024]{1,0:T(8,128)(2,1)S(1)}, bf16[48,1024]{1,0:T(8,128)(2,1)S(1)}, u32[]{:S(2)}, u32[]{:S(2)}) %collective-permute-start.28) | collective-permute-done | bytes 98336 | tf_op jit(solution)/shard_map/ppermute | solution.py:96
  192.1 0.9 slice_add_fusion.6
  193.1 3.3 %collective-permute-done.25 = bf16[48,2048]{1,0:T(8,128)(2,1)S(1)} collective-permute-done((bf16[48,2048]{1,0:T(8,128)(2,1)S(1)}, bf16[48,2048]{1,0:T(8,128)(2,1)S(1)}, u32[]{:S(2)}, u32[]{:S(2)}) %collective-permute-start.25) | collective-permute-done | bytes 196640 | tf_op jit(solution)/shard_map/ppermute | solution.py:96
  196.4 3.8 %collective-permute-start.26 = (bf16[48,2048]{1,0:T(8,128)(2,1)S(1)}, bf16[48,2048]{1,0:T(8,128)(2,1)S(1)}, u32[]{:S(2)}, u32[]{:S(2)}) collective-permute-start(bf16[48,2048]{1,0:T(8,128)(2,1)S(1)} %slice_add_fusion.2), channel_id=1, source_target_pairs={{0,2},{2,4},{4,6},{6,8},{8,10},{10,12},{12,14},{14,0},{1,3},{3,5},... | collective-permute-start | bytes 589832 | tf_op jit(solution)/shard_map/ppermute | solution.py:96
  200.2 4.4 %collective-permute-done.29 = bf16[48,2048]{1,0:T(8,128)(2,1)S(1)} collective-permute-done((bf16[48,2048]{1,0:T(8,128)(2,1)S(1)}, bf16[48,2048]{1,0:T(8,128)(2,1)S(1)}, u32[]{:S(2)}, u32[]{:S(2)}) %collective-permute-start.29) | collective-permute-done | bytes 196640 | tf_op jit(solution)/shard_map/ppermute | solution.py:96
  204.6 4.0 %collective-permute-done.26 = bf16[48,2048]{1,0:T(8,128)(2,1)S(1)} collective-permute-done((bf16[48,2048]{1,0:T(8,128)(2,1)S(1)}, bf16[48,2048]{1,0:T(8,128)(2,1)S(1)}, u32[]{:S(2)}, u32[]{:S(2)}) %collective-permute-start.26) | collective-permute-done | bytes 196640 | tf_op jit(solution)/shard_map/ppermute | solution.py:96
  208.7 3.8 %collective-permute-start.27 = (bf16[48,2048]{1,0:T(8,128)(2,1)S(1)}, bf16[48,2048]{1,0:T(8,128)(2,1)S(1)}, u32[]{:S(2)}, u32[]{:S(2)}) collective-permute-start(bf16[48,2048]{1,0:T(8,128)(2,1)S(1)} %get-tuple-element.25), channel_id=1, source_target_pairs={{0,2},{2,4},{4,6},{6,8},{8,10},{10,12},{12,14},{14,0},{1,3},{3,5},... | collective-permute-start | bytes 589832 | tf_op jit(solution)/shard_map/ppermute | solution.py:96
  212.5 8.2 %collective-permute-done.30 = bf16[48,2048]{1,0:T(8,128)(2,1)S(1)} collective-permute-done((bf16[48,2048]{1,0:T(8,128)(2,1)S(1)}, bf16[48,2048]{1,0:T(8,128)(2,1)S(1)}, u32[]{:S(2)}, u32[]{:S(2)}) %collective-permute-start.30) | collective-permute-done | bytes 196640 | tf_op jit(solution)/shard_map/ppermute | solution.py:96
  220.8 11.5 %collective-permute-done.31 = bf16[48,2048]{1,0:T(8,128)(2,1)S(1)} collective-permute-done((bf16[48,2048]{1,0:T(8,128)(2,1)S(1)}, bf16[48,2048]{1,0:T(8,128)(2,1)S(1)}, u32[]{:S(2)}, u32[]{:S(2)}) %collective-permute-start.31) | collective-permute-done | bytes 196640 | tf_op jit(solution)/shard_map/ppermute | solution.py:96
  232.4 0.8 reshape.167
  233.1 5.1 %all-to-all-start.2 = ((bf16[16,48,128]{2,1,0:T(8,128)(2,1)}), bf16[16,48,128]{2,1,0:T(8,128)(2,1)S(1)}, u32[]{:S(2)}, u32[]{:S(2)}) async-start(bf16[16,48,128]{2,1,0:T(8,128)(2,1)} %reshape.167), calls=%async_computation.4 | async-start | bytes 393216 | tf_op jit(solution)/shard_map/all_to_all | solution.py:316
  238.4 1.2 reshape.166
  239.6 7.0 %all-to-all-done.2 = bf16[16,48,128]{2,1,0:T(8,128)(2,1)S(1)} async-done(((bf16[16,48,128]{2,1,0:T(8,128)(2,1)}), bf16[16,48,128]{2,1,0:T(8,128)(2,1)S(1)}, u32[]{:S(2)}, u32[]{:S(2)}) %all-to-all-start.2) | async-done | bytes 196640 | tf_op jit(solution)/shard_map/all_to_all | solution.py:316
  246.6 12.7 %all_to_all.16 = bf16[16,112,128]{2,1,0:T(8,128)(2,1)S(1)} all-to-all(bf16[16,112,128]{2,1,0:T(8,128)(2,1)S(1)} %reshape.166), channel_id=1, replica_groups=mesh['sp'=16,'tp_0'=8,'tp_1'=2] {'sp'}, dimensions={0} | all-to-all | bytes 917504 | tf_op jit(solution)/shard_map/all_to_all | solution.py:316
  259.7 1.1 fusion.1
  (115 shorter events, 7.6 us)
Async XLA Ops:
  6.5 72.5 %reduce-scatter.3.cloned.1.call-start = ((), (), s32[]{:S(2)}) async-start(), calls=%async_computation.5 | async-start | bytes 2949120 | tf_op jit(solution)/shard_map/reduce_scatter | solution.py:300
  6.5 7.3 %copy-start.2 = (bf16[2048,128]{1,0:T(8,128)(2,1)S(1)}, bf16[2048,128]{1,0:T(8,128)(2,1)}, u32[]{:S(2)}) copy-start(bf16[2048,128]{1,0:T(8,128)(2,1)} %param.14) | copy-start | bytes 1572868
  6.5 7.9 %copy-start = (bf16[128,2048]{1,0:T(8,128)(2,1)S(1)}, bf16[128,2048]{1,0:T(8,128)(2,1)}, u32[]{:S(2)}) copy-start(bf16[128,2048]{1,0:T(8,128)(2,1)} %param.18) | copy-start | bytes 1572868
  7.9 8.9 %collective-permute-start.2 = (bf16[2,128,128]{2,1,0:T(8,128)(2,1)S(1)}, bf16[2,128,128]{2,1,0:T(8,128)(2,1)S(1)}, u32[]{:S(2)}, u32[]{:S(2)}) collective-permute-start(bf16[2,128,128]{2,1,0:T(8,128)(2,1)S(1)} %get-tuple-element.40), channel_id=1, source_target_pairs={{16,0},{32,16},{48,32},{64,48},{80,64},{96,80},{112,96},{128,112},... | collective-permute-start | bytes 196616 | tf_op jit(solution)/shard_map/ppermute | solution.py:33
  9.2 7.6 %collective-permute-start.1 = (bf16[2,128,128]{2,1,0:T(8,128)(2,1)S(1)}, bf16[2,128,128]{2,1,0:T(8,128)(2,1)S(1)}, u32[]{:S(2)}, u32[]{:S(2)}) collective-permute-start(bf16[2,128,128]{2,1,0:T(8,128)(2,1)S(1)} %get-tuple-element.39), channel_id=1, source_target_pairs={{0,16},{16,32},{32,48},{48,64},{64,80},{80,96},{96,112},{112,128},... | collective-permute-start | bytes 196616 | tf_op jit(solution)/shard_map/ppermute | solution.py:32
  13.9 3.6 %collective-permute-start = (bf16[8,1,128,128]{3,2,1,0:T(8,128)(2,1)S(1)}, bf16[8,1,128,128]{3,2,1,0:T(8,128)(2,1)S(1)}, u32[]{:S(2)}, u32[]{:S(2)}) collective-permute-start(bf16[8,1,128,128]{3,2,1,0:T(8,128)(2,1)S(1)} %get-tuple-element.42), channel_id=1, source_target_pairs={{0,1},{1,0},{2,3},{3,2},{4,5},{5,4},{6,7},{7,6},{8,9},{9,8},{10,11... | collective-permute-start | bytes 786440 | tf_op jit(solution)/shard_map/ppermute | solution.py:46
  14.0 2.1 collective-permute-start.3
  14.5 6.6 %collective-permute-start.4 = (bf16[128,2048]{1,0:T(8,128)(2,1)S(1)}, bf16[128,2048]{1,0:T(8,128)(2,1)S(1)}, u32[]{:S(2)}, u32[]{:S(2)}) collective-permute-start(bf16[128,2048]{1,0:T(8,128)(2,1)S(1)} %copy-done), channel_id=1, source_target_pairs={{0,1},{1,0},{2,3},{3,2},{4,5},{5,4},{6,7},{7,6},{8,9},{9,8},{10,11... | collective-permute-start | bytes 1572872 | tf_op jit(solution)/shard_map/ppermute | solution.py:290
  23.5 137.5 %all-gather.2.cloned.1.call-start = ((), (), s32[]{:S(2)}) async-start(), calls=%async_computation.6 | async-start | bytes 4386816 | tf_op jit(solution)/shard_map/all_gather | solution.py:330
  23.5 56.6 %collective-permute-start.13 = (bf16[3,2048,128]{2,1,0:T(8,128)(2,1)}, bf16[3,2048,128]{2,1,0:T(8,128)(2,1)}, u32[]{:S(2)}, u32[]{:S(2)}) collective-permute-start(bf16[3,2048,128]{2,1,0:T(8,128)(2,1)} %refs_0_.1), channel_id=1, source_target_pairs={{0,1},{1,0},{2,3},{3,2},{4,5},{5,4},{6,7},{7,6},{8,9},{9,8},{10,11... | collective-permute-start | bytes 4718600 | tf_op jit(solution)/shard_map/ppermute | solution.py:264
  24.0 56.1 %collective-permute-start.14 = (bf16[3,2048,128]{2,1,0:T(8,128)(2,1)}, bf16[3,2048,128]{2,1,0:T(8,128)(2,1)}, u32[]{:S(2)}, u32[]{:S(2)}) collective-permute-start(bf16[3,2048,128]{2,1,0:T(8,128)(2,1)} %refs_2_.1), channel_id=1, source_target_pairs={{0,1},{1,0},{2,3},{3,2},{4,5},{5,4},{6,7},{7,6},{8,9},{9,8},{10,11... | collective-permute-start | bytes 4718600 | tf_op jit(solution)/shard_map/ppermute | solution.py:264
  24.1 56.0 %collective-permute-start.15 = (bf16[3,128,2048]{2,1,0:T(8,128)(2,1)}, bf16[3,128,2048]{2,1,0:T(8,128)(2,1)}, u32[]{:S(2)}, u32[]{:S(2)}) collective-permute-start(bf16[3,128,2048]{2,1,0:T(8,128)(2,1)} %refs_4_.1), channel_id=1, source_target_pairs={{0,1},{1,0},{2,3},{3,2},{4,5},{5,4},{6,7},{7,6},{8,9},{9,8},{10,11... | collective-permute-start | bytes 4718600 | tf_op jit(solution)/shard_map/ppermute | solution.py:264
  24.5 3.9 %copy-start.6 = (s32[128]{0:T(128)S(1)}, s32[128]{0:T(128)}, u32[]{:S(2)}) copy-start(s32[128]{0:T(128)} %param.22) | copy-start | bytes 1540
  24.5 4.0 %copy-start.8 = (bf16[128,2]{0,1:T(2,128)(2,1)S(1)}, bf16[128,2]{0,1:T(2,128)(2,1)}, u32[]{:S(2)}) copy-start(bf16[128,2]{0,1:T(2,128)(2,1)} %param.24) | copy-start | bytes 1540
  25.2 16.8 %copy-start.7 = (s32[128,2]{0,1:T(2,128)S(1)}, s32[128,2]{0,1:T(2,128)}, u32[]{:S(2)}) copy-start(s32[128,2]{0,1:T(2,128)} %param.23) | copy-start | bytes 3076
  25.2 5.5 %collective-permute-start.5 = (bf16[128,384]{1,0:T(8,128)(2,1)S(1)}, bf16[128,384]{1,0:T(8,128)(2,1)S(1)}, u32[]{:S(2)}, u32[]{:S(2)}) collective-permute-start(bf16[128,384]{1,0:T(8,128)(2,1)S(1)} %get-tuple-element.47), channel_id=1, source_target_pairs={{0,2},{2,4},{4,6},{6,8},{8,10},{10,12},{12,14},{14,0},{1,3},{3,5},... | collective-permute-start | bytes 294920 | tf_op jit(solution)/shard_map/ppermute | solution.py:96
  28.5 6.0 %collective-permute-start.9 = (bf16[128,384]{1,0:T(8,128)(2,1)S(1)}, bf16[128,384]{1,0:T(8,128)(2,1)S(1)}, u32[]{:S(2)}, u32[]{:S(2)}) collective-permute-start(bf16[128,384]{1,0:T(8,128)(2,1)S(1)} %get-tuple-element.48), channel_id=1, source_target_pairs={{0,14},{2,0},{4,2},{6,4},{8,6},{10,8},{12,10},{14,12},{1,15},{3,1}... | collective-permute-start | bytes 294920 | tf_op jit(solution)/shard_map/ppermute | solution.py:96
  30.8 7.4 %collective-permute-start.6 = (bf16[128,768]{1,0:T(8,128)(2,1)S(1)}, bf16[128,768]{1,0:T(8,128)(2,1)S(1)}, u32[]{:S(2)}, u32[]{:S(2)}) collective-permute-start(bf16[128,768]{1,0:T(8,128)(2,1)S(1)} %pad_maximum_fusion.5), channel_id=1, source_target_pairs={{0,2},{2,4},{4,6},{6,8},{8,10},{10,12},{12,14},{14,0},{1,3},{3,5},... | collective-permute-start | bytes 589832 | tf_op jit(solution)/shard_map/ppermute | solution.py:96
  34.6 7.8 %collective-permute-start.10 = (bf16[128,768]{1,0:T(8,128)(2,1)S(1)}, bf16[128,768]{1,0:T(8,128)(2,1)S(1)}, u32[]{:S(2)}, u32[]{:S(2)}) collective-permute-start(bf16[128,768]{1,0:T(8,128)(2,1)S(1)} %pad_maximum_fusion.6), channel_id=1, source_target_pairs={{0,14},{2,0},{4,2},{6,4},{8,6},{10,8},{12,10},{14,12},{1,15},{3,1}... | collective-permute-start | bytes 589832 | tf_op jit(solution)/shard_map/ppermute | solution.py:96
  38.2 11.6 %collective-permute-start.7 = (bf16[128,768]{1,0:T(8,128)(2,1)S(1)}, bf16[128,768]{1,0:T(8,128)(2,1)S(1)}, u32[]{:S(2)}, u32[]{:S(2)}) collective-permute-start(bf16[128,768]{1,0:T(8,128)(2,1)S(1)} %bitcast_add_fusion.2), channel_id=1, source_target_pairs={{0,2},{2,4},{4,6},{6,8},{8,10},{10,12},{12,14},{14,0},{1,3},{3,5},... | collective-permute-start | bytes 589832 | tf_op jit(solution)/shard_map/ppermute | solution.py:96
  49.8 12.3 %collective-permute-start.11 = (bf16[128,768]{1,0:T(8,128)(2,1)S(1)}, bf16[128,768]{1,0:T(8,128)(2,1)S(1)}, u32[]{:S(2)}, u32[]{:S(2)}) collective-permute-start(bf16[128,768]{1,0:T(8,128)(2,1)S(1)} %get-tuple-element.32), channel_id=1, source_target_pairs={{0,14},{2,0},{4,2},{6,4},{8,6},{10,8},{12,10},{14,12},{1,15},{3,1}... | collective-permute-start | bytes 589832 | tf_op jit(solution)/shard_map/ppermute | solution.py:96
  49.9 12.6 %collective-permute-start.8 = (bf16[128,768]{1,0:T(8,128)(2,1)S(1)}, bf16[128,768]{1,0:T(8,128)(2,1)S(1)}, u32[]{:S(2)}, u32[]{:S(2)}) collective-permute-start(bf16[128,768]{1,0:T(8,128)(2,1)S(1)} %get-tuple-element.31), channel_id=1, source_target_pairs={{0,2},{2,4},{4,6},{6,8},{8,10},{10,12},{12,14},{14,0},{1,3},{3,5},... | collective-permute-start | bytes 589832 | tf_op jit(solution)/shard_map/ppermute | solution.py:96
  62.2 11.6 %collective-permute-start.12 = (bf16[128,768]{1,0:T(8,128)(2,1)S(1)}, bf16[128,768]{1,0:T(8,128)(2,1)S(1)}, u32[]{:S(2)}, u32[]{:S(2)}) collective-permute-start(bf16[128,768]{1,0:T(8,128)(2,1)S(1)} %bitcast_add_fusion.1), channel_id=1, source_target_pairs={{0,14},{2,0},{4,2},{6,4},{8,6},{10,8},{12,10},{14,12},{1,15},{3,1}... | collective-permute-start | bytes 589832 | tf_op jit(solution)/shard_map/ppermute | solution.py:96
  62.5 17.9 %copy-start.3 = (bf16[128,2048]{1,0:T(8,128)(2,1)S(1)}, bf16[128,2048]{1,0:T(8,128)(2,1)}, u32[]{:S(2)}) copy-start(bf16[128,2048]{1,0:T(8,128)(2,1)} %param.19) | copy-start | bytes 1572868
  62.5 17.8 %copy-start.4 = (f32[2048]{0:T(1024)S(1)}, f32[2048]{0:T(1024)}, u32[]{:S(2)}) copy-start(f32[2048]{0:T(1024)} %param.20) | copy-start | bytes 24580
  80.1 0.7 copy-start.5
  102.1 136.3 %reduce-scatter.5.cloned.1.call-start = ((), (), s32[]{:S(2)}) async-start(), calls=%async_computation.7 | async-start | bytes 4128768 | tf_op jit(solution)/shard_map/reduce_scatter | solution.py:335
  103.6 6.8 %collective-permute-start.16 = (bf16[48,2176]{1,0:T(8,128)(2,1)S(1)}, bf16[48,2176]{1,0:T(8,128)(2,1)S(1)}, u32[]{:S(2)}, u32[]{:S(2)}) collective-permute-start(bf16[48,2176]{1,0:T(8,128)(2,1)S(1)} %get-tuple-element.51), channel_id=1, source_target_pairs={{0,2},{2,4},{4,6},{6,8},{8,10},{10,12},{12,14},{14,0},{1,3},{3,5},... | collective-permute-start | bytes 626696 | tf_op jit(solution)/shard_map/ppermute | solution.py:96
  105.1 7.0 %collective-permute-start.17 = (bf16[48,2176]{1,0:T(8,128)(2,1)S(1)}, bf16[48,2176]{1,0:T(8,128)(2,1)S(1)}, u32[]{:S(2)}, u32[]{:S(2)}) collective-permute-start(bf16[48,2176]{1,0:T(8,128)(2,1)S(1)} %get-tuple-element.51), channel_id=1, source_target_pairs={{0,14},{2,0},{4,2},{6,4},{8,6},{10,8},{12,10},{14,12},{1,15},{3,1}... | collective-permute-start | bytes 626696 | tf_op jit(solution)/shard_map/ppermute | solution.py:96
  110.4 11.4 %collective-permute-start.18 = (bf16[48,2176]{1,0:T(8,128)(2,1)S(1)}, bf16[48,2176]{1,0:T(8,128)(2,1)S(1)}, u32[]{:S(2)}, u32[]{:S(2)}) collective-permute-start(bf16[48,2176]{1,0:T(8,128)(2,1)S(1)} %collective-permute-done.16), channel_id=1, source_target_pairs={{0,2},{2,4},{4,6},{6,8},{8,10},{10,12},{12,14},{14,0},{1,3},{3,5},... | collective-permute-start | bytes 626696 | tf_op jit(solution)/shard_map/ppermute | solution.py:96
  112.1 12.4 %collective-permute-start.19 = (bf16[48,2176]{1,0:T(8,128)(2,1)S(1)}, bf16[48,2176]{1,0:T(8,128)(2,1)S(1)}, u32[]{:S(2)}, u32[]{:S(2)}) collective-permute-start(bf16[48,2176]{1,0:T(8,128)(2,1)S(1)} %collective-permute-done.17), channel_id=1, source_target_pairs={{0,14},{2,0},{4,2},{6,4},{8,6},{10,8},{12,10},{14,12},{1,15},{3,1}... | collective-permute-start | bytes 626696 | tf_op jit(solution)/shard_map/ppermute | solution.py:96
  121.8 15.1 %collective-permute-start.20 = (bf16[48,2176]{1,0:T(8,128)(2,1)S(1)}, bf16[48,2176]{1,0:T(8,128)(2,1)S(1)}, u32[]{:S(2)}, u32[]{:S(2)}) collective-permute-start(bf16[48,2176]{1,0:T(8,128)(2,1)S(1)} %collective-permute-done.18), channel_id=1, source_target_pairs={{0,2},{2,4},{4,6},{6,8},{8,10},{10,12},{12,14},{14,0},{1,3},{3,5},... | collective-permute-start | bytes 626696 | tf_op jit(solution)/shard_map/ppermute | solution.py:96
  124.5 12.3 %collective-permute-start.21 = (bf16[48,2176]{1,0:T(8,128)(2,1)S(1)}, bf16[48,2176]{1,0:T(8,128)(2,1)S(1)}, u32[]{:S(2)}, u32[]{:S(2)}) collective-permute-start(bf16[48,2176]{1,0:T(8,128)(2,1)S(1)} %collective-permute-done.19), channel_id=1, source_target_pairs={{0,14},{2,0},{4,2},{6,4},{8,6},{10,8},{12,10},{14,12},{1,15},{3,1}... | collective-permute-start | bytes 626696 | tf_op jit(solution)/shard_map/ppermute | solution.py:96
  136.8 8.5 %collective-permute-start.23 = (bf16[48,1152]{1,0:T(8,128)(2,1)S(1)}, bf16[48,1152]{1,0:T(8,128)(2,1)S(1)}, u32[]{:S(2)}, u32[]{:S(2)}) collective-permute-start(bf16[48,1152]{1,0:T(8,128)(2,1)S(1)} %slice.152), channel_id=1, source_target_pairs={{0,14},{2,0},{4,2},{6,4},{8,6},{10,8},{12,10},{14,12},{1,15},{3,1}... | collective-permute-start | bytes 331784 | tf_op jit(solution)/shard_map/ppermute | solution.py:96
  137.0 7.9 %collective-permute-start.22 = (bf16[48,1024]{1,0:T(8,128)(2,1)S(1)}, bf16[48,1024]{1,0:T(8,128)(2,1)S(1)}, u32[]{:S(2)}, u32[]{:S(2)}) collective-permute-start(bf16[48,1024]{1,0:T(8,128)(2,1)S(1)} %slice.151), channel_id=1, source_target_pairs={{0,2},{2,4},{4,6},{6,8},{8,10},{10,12},{12,14},{14,0},{1,3},{3,5},... | collective-permute-start | bytes 294920 | tf_op jit(solution)/shard_map/ppermute | solution.py:96
  177.6 18.7 %copy-start.1 = (bf16[384,2048]{1,0:T(8,128)(2,1)S(1)}, bf16[384,2048]{1,0:T(8,128)(2,1)}, u32[]{:S(2)}) copy-start(bf16[384,2048]{1,0:T(8,128)(2,1)} %experts.2) | copy-start | bytes 4718596
  178.7 4.6 %collective-permute-start.24 = (bf16[48,1024]{1,0:T(8,128)(2,1)S(1)}, bf16[48,1024]{1,0:T(8,128)(2,1)S(1)}, u32[]{:S(2)}, u32[]{:S(2)}) collective-permute-start(bf16[48,1024]{1,0:T(8,128)(2,1)S(1)} %slice.130), channel_id=1, source_target_pairs={{0,2},{2,4},{4,6},{6,8},{8,10},{10,12},{12,14},{14,0},{1,3},{3,5},... | collective-permute-start | bytes 294920 | tf_op jit(solution)/shard_map/ppermute | solution.py:96
  184.3 7.7 %collective-permute-start.28 = (bf16[48,1024]{1,0:T(8,128)(2,1)S(1)}, bf16[48,1024]{1,0:T(8,128)(2,1)S(1)}, u32[]{:S(2)}, u32[]{:S(2)}) collective-permute-start(bf16[48,1024]{1,0:T(8,128)(2,1)S(1)} %get-tuple-element.28), channel_id=1, source_target_pairs={{0,14},{2,0},{4,2},{6,4},{8,6},{10,8},{12,10},{14,12},{1,15},{3,1}... | collective-permute-start | bytes 294920 | tf_op jit(solution)/shard_map/ppermute | solution.py:96
  184.5 11.9 %collective-permute-start.25 = (bf16[48,2048]{1,0:T(8,128)(2,1)S(1)}, bf16[48,2048]{1,0:T(8,128)(2,1)S(1)}, u32[]{:S(2)}, u32[]{:S(2)}) collective-permute-start(bf16[48,2048]{1,0:T(8,128)(2,1)S(1)} %pad_maximum_fusion.7), channel_id=1, source_target_pairs={{0,2},{2,4},{4,6},{6,8},{8,10},{10,12},{12,14},{14,0},{1,3},{3,5},... | collective-permute-start | bytes 589832 | tf_op jit(solution)/shard_map/ppermute | solution.py:96
  193.0 11.6 %collective-permute-start.29 = (bf16[48,2048]{1,0:T(8,128)(2,1)S(1)}, bf16[48,2048]{1,0:T(8,128)(2,1)S(1)}, u32[]{:S(2)}, u32[]{:S(2)}) collective-permute-start(bf16[48,2048]{1,0:T(8,128)(2,1)S(1)} %pad_maximum_fusion.8), channel_id=1, source_target_pairs={{0,14},{2,0},{4,2},{6,4},{8,6},{10,8},{12,10},{14,12},{1,15},{3,1}... | collective-permute-start | bytes 589832 | tf_op jit(solution)/shard_map/ppermute | solution.py:96
  196.4 12.2 %collective-permute-start.26 = (bf16[48,2048]{1,0:T(8,128)(2,1)S(1)}, bf16[48,2048]{1,0:T(8,128)(2,1)S(1)}, u32[]{:S(2)}, u32[]{:S(2)}) collective-permute-start(bf16[48,2048]{1,0:T(8,128)(2,1)S(1)} %slice_add_fusion.2), channel_id=1, source_target_pairs={{0,2},{2,4},{4,6},{6,8},{8,10},{10,12},{12,14},{14,0},{1,3},{3,5},... | collective-permute-start | bytes 589832 | tf_op jit(solution)/shard_map/ppermute | solution.py:96
  208.6 12.1 %collective-permute-start.30 = (bf16[48,2048]{1,0:T(8,128)(2,1)S(1)}, bf16[48,2048]{1,0:T(8,128)(2,1)S(1)}, u32[]{:S(2)}, u32[]{:S(2)}) collective-permute-start(bf16[48,2048]{1,0:T(8,128)(2,1)S(1)} %get-tuple-element.26), channel_id=1, source_target_pairs={{0,14},{2,0},{4,2},{6,4},{8,6},{10,8},{12,10},{14,12},{1,15},{3,1}... | collective-permute-start | bytes 589832 | tf_op jit(solution)/shard_map/ppermute | solution.py:96
  208.7 12.1 %collective-permute-start.27 = (bf16[48,2048]{1,0:T(8,128)(2,1)S(1)}, bf16[48,2048]{1,0:T(8,128)(2,1)S(1)}, u32[]{:S(2)}, u32[]{:S(2)}) collective-permute-start(bf16[48,2048]{1,0:T(8,128)(2,1)S(1)} %get-tuple-element.25), channel_id=1, source_target_pairs={{0,2},{2,4},{4,6},{6,8},{8,10},{10,12},{12,14},{14,0},{1,3},{3,5},... | collective-permute-start | bytes 589832 | tf_op jit(solution)/shard_map/ppermute | solution.py:96
  220.7 11.6 %collective-permute-start.31 = (bf16[48,2048]{1,0:T(8,128)(2,1)S(1)}, bf16[48,2048]{1,0:T(8,128)(2,1)S(1)}, u32[]{:S(2)}, u32[]{:S(2)}) collective-permute-start(bf16[48,2048]{1,0:T(8,128)(2,1)S(1)} %slice_add_fusion.1), channel_id=1, source_target_pairs={{0,14},{2,0},{4,2},{6,4},{8,6},{10,8},{12,10},{14,12},{1,15},{3,1}... | collective-permute-start | bytes 589832 | tf_op jit(solution)/shard_map/ppermute | solution.py:96
  233.1 13.5 %all-to-all-start.2 = ((bf16[16,48,128]{2,1,0:T(8,128)(2,1)}), bf16[16,48,128]{2,1,0:T(8,128)(2,1)S(1)}, u32[]{:S(2)}, u32[]{:S(2)}) async-start(bf16[16,48,128]{2,1,0:T(8,128)(2,1)} %reshape.167), calls=%async_computation.4 | async-start | bytes 393216 | tf_op jit(solution)/shard_map/all_to_all | solution.py:316
Sparse Core Ops, SparseCore 0:
  23.6 55.3 reduce-scatter.2
  102.2 58.7 all-gather.1
  177.7 60.6 reduce-scatter.4

commit v2 on v0

--- a/solution.py
+++ b/solution.py
@@ -148,21 +148,30 @@
     def out_copy(i):
         return pltpu.make_async_copy(out.at[span(i)], out_to.at[span(i)], out_sems.at[i])
 
+    row_copy(0).start()
     for k in range(4):
         weight_copy(k, 0).start()
-    for i in range(steps):
-        row_copy(i).start()
-    for e in range(1, GROUP_EXPERTS):
-        for k in range(4):
-            weight_copy(k, e).start()
-    for e in range(GROUP_EXPERTS):
-        for k in (4, 5):
-            weight_copy(k, e).start()
 
     @pl.loop(0, GROUP_EXPERTS)
     def _(e):
         for k in range(4):
             weight_copy(k, e).wait()
+
+        @pl.when(e == 0)
+        def _():
+            for i in range(1, steps):
+                row_copy(i).start()
+
+        @pl.when(e + 1 < GROUP_EXPERTS)
+        def _():
+            for k in range(4):
+                weight_copy(k, e + 1).start()
+
+        @pl.when(e == 1)
+        def _():
+            for member in range(GROUP_EXPERTS):
+                for k in (4, 5):
+                    weight_copy(k, member).start()
 
         @pl.loop(0, steps)
         def _(i):

time: 268 us -> 267 us (level)
  no operation moved by 1% of the time
where the time goes in v2:
time: 267 us; the launch traced here: 266 us
  waiting for transfers between devices  118 us (44%)
  starting transfers between devices  49.3 us (18%)
  blocking collectives  32.1 us (12%)
  Pallas kernels  25.1 us (9%)
  between operations  14.5 us (5%)
  local copies, waits for them, and re-layouts  11.6 us (4%)
  other arithmetic  9.21 us (3%)
  matrix products  6.81 us (3%)
    ppermute x12, waiting for transfers between devices, shifts(): lax.ppermute(a, Z, down)  59.7 us
    ppermute x12, waiting for transfers between devices, shifts(): lax.ppermute(a, Z, up)  40.3 us
    ppermute x12, starting transfers between devices, shifts(): lax.ppermute(a, Z, up)  34.7 us
    all_to_all x2, blocking collectives, exchange(): lax.all_to_all(rows.reshape(groups, -1, LANES), 'sp', split_axis=0, conca...  32.1 us
    pallas_call x2, Pallas kernels, experts(): pl.pallas_call(experts_kernel, in_specs=[anywhere] * 7, out_specs=anywher...  25.1 us
    all_to_all x1, waiting for transfers between devices, exchange(): lax.all_to_all(rows.reshape(groups, -1, LANES), 'sp', split_axis=0, conca...  6.96 us
    all_gather x1, waiting for transfers between devices, per_device(): pool_a = lax.all_gather(with_gates(0, cap_a), Z, axis=0, tiled=True)  5.48 us
  transfers between devices with their start and end apart: 36, of which 21 were waited for; matrix products, arithmetic and copies ran while one was open for 7% of the time, Pallas kernels for 4%

profile of v2, /device:TPU:96, one launch (start us, length us, event | category | flops | bytes accessed | tf_op | source)
XLA Modules:
  0.0 266.5 jit_solution(9880283170983687617)
XLA Ops:
  6.5 1.4 dynamic-slice_bitcast_fusion
  7.9 1.3 collective-permute-start.2
  9.2 4.5 %collective-permute-start.1 = (bf16[2,128,128]{2,1,0:T(8,128)(2,1)S(1)}, bf16[2,128,128]{2,1,0:T(8,128)(2,1)S(1)}, u32[]{:S(2)}, u32[]{:S(2)}) collective-permute-start(bf16[2,128,128]{2,1,0:T(8,128)(2,1)S(1)} %get-tuple-element.39), channel_id=1, source_target_pairs={{0,16},{16,32},{32,48},{48,64},{64,80},{80,96},{96,112},{112,128},... | collective-permute-start | bytes 196616 | tf_op jit(solution)/shard_map/ppermute | solution.py:32
  15.4 0.6 fusion.4
  16.1 0.7 pad_maximum_fusion.11
  17.4 0.9 fusion
  18.4 1.3 fusion.2
  19.7 1.3 fusion.7
  21.1 2.3 bitcast_convert_fusion
  24.5 0.6 bitcast_convert_fusion.1
  25.2 3.2 %collective-permute-start.5 = (bf16[128,384]{1,0:T(8,128)(2,1)S(1)}, bf16[128,384]{1,0:T(8,128)(2,1)S(1)}, u32[]{:S(2)}, u32[]{:S(2)}) collective-permute-start(bf16[128,384]{1,0:T(8,128)(2,1)S(1)} %get-tuple-element.47), channel_id=1, source_target_pairs={{0,2},{2,4},{4,6},{6,8},{8,10},{10,12},{12,14},{14,0},{1,3},{3,5},... | collective-permute-start | bytes 294920 | tf_op jit(solution)/shard_map/ppermute | solution.py:96
  28.6 2.1 collective-permute-done.5
  30.8 3.8 %collective-permute-start.6 = (bf16[128,768]{1,0:T(8,128)(2,1)S(1)}, bf16[128,768]{1,0:T(8,128)(2,1)S(1)}, u32[]{:S(2)}, u32[]{:S(2)}) collective-permute-start(bf16[128,768]{1,0:T(8,128)(2,1)S(1)} %pad_maximum_fusion.5), channel_id=1, source_target_pairs={{0,2},{2,4},{4,6},{6,8},{8,10},{10,12},{12,14},{14,0},{1,3},{3,5},... | collective-permute-start | bytes 589832 | tf_op jit(solution)/shard_map/ppermute | solution.py:96
  34.9 3.3 %collective-permute-done.6 = bf16[128,768]{1,0:T(8,128)(2,1)S(1)} collective-permute-done((bf16[128,768]{1,0:T(8,128)(2,1)S(1)}, bf16[128,768]{1,0:T(8,128)(2,1)S(1)}, u32[]{:S(2)}, u32[]{:S(2)}) %collective-permute-start.6) | collective-permute-done | bytes 196640 | tf_op jit(solution)/shard_map/ppermute | solution.py:96
  38.2 3.8 %collective-permute-start.7 = (bf16[128,768]{1,0:T(8,128)(2,1)S(1)}, bf16[128,768]{1,0:T(8,128)(2,1)S(1)}, u32[]{:S(2)}, u32[]{:S(2)}) collective-permute-start(bf16[128,768]{1,0:T(8,128)(2,1)S(1)} %bitcast_add_fusion.2), channel_id=1, source_target_pairs={{0,2},{2,4},{4,6},{6,8},{8,10},{10,12},{12,14},{14,0},{1,3},{3,5},... | collective-permute-start | bytes 589832 | tf_op jit(solution)/shard_map/ppermute | solution.py:96
  42.4 7.4 %collective-permute-done.7 = bf16[128,768]{1,0:T(8,128)(2,1)S(1)} collective-permute-done((bf16[128,768]{1,0:T(8,128)(2,1)S(1)}, bf16[128,768]{1,0:T(8,128)(2,1)S(1)}, u32[]{:S(2)}, u32[]{:S(2)}) %collective-permute-start.7) | collective-permute-done | bytes 196640 | tf_op jit(solution)/shard_map/ppermute | solution.py:96
  49.9 3.8 %collective-permute-start.8 = (bf16[128,768]{1,0:T(8,128)(2,1)S(1)}, bf16[128,768]{1,0:T(8,128)(2,1)S(1)}, u32[]{:S(2)}, u32[]{:S(2)}) collective-permute-start(bf16[128,768]{1,0:T(8,128)(2,1)S(1)} %get-tuple-element.31), channel_id=1, source_target_pairs={{0,2},{2,4},{4,6},{6,8},{8,10},{10,12},{12,14},{14,0},{1,3},{3,5},... | collective-permute-start | bytes 589832 | tf_op jit(solution)/shard_map/ppermute | solution.py:96
  53.7 8.5 %collective-permute-done.11 = bf16[128,768]{1,0:T(8,128)(2,1)S(1)} collective-permute-done((bf16[128,768]{1,0:T(8,128)(2,1)S(1)}, bf16[128,768]{1,0:T(8,128)(2,1)S(1)}, u32[]{:S(2)}, u32[]{:S(2)}) %collective-permute-start.11) | collective-permute-done | bytes 196640 | tf_op jit(solution)/shard_map/ppermute | solution.py:96
  62.5 11.3 %collective-permute-done.12 = bf16[128,768]{1,0:T(8,128)(2,1)S(1)} collective-permute-done((bf16[128,768]{1,0:T(8,128)(2,1)S(1)}, bf16[128,768]{1,0:T(8,128)(2,1)S(1)}, u32[]{:S(2)}, u32[]{:S(2)}) %collective-permute-start.12) | collective-permute-done | bytes 196640 | tf_op jit(solution)/shard_map/ppermute | solution.py:96
  73.8 5.2 %reduce-scatter.3.cloned.1.call-done = bf16[128,1280]{1,0:T(8,128)(2,1)} async-done(((bf16[1024,1280]{1,0:T(8,128)(2,1)}), bf16[128,1280]{1,0:T(8,128)(2,1)}) %reduce-scatter.3.cloned.1.call-update) | async-done | bytes 327696 | tf_op jit(solution)/shard_map/reduce_scatter | solution.py:309
  79.0 1.1 maximum_convert_fusion
  81.6 19.4 %all_to_all.15 = bf16[16,176,128]{2,1,0:T(8,128)(2,1)S(1)} all-to-all(bf16[16,176,128]{2,1,0:T(8,128)(2,1)S(1)} %fusion.12), channel_id=1, replica_groups=mesh['sp'=16,'tp_0'=8,'tp_1'=2] {'sp'}, dimensions={0} | all-to-all | bytes 1441792 | tf_op jit(solution)/shard_map/all_to_all | solution.py:325
  101.2 0.8 pad_maximum_fusion.3
  102.3 0.7 constant_dynamic-update-slice_fusion.1
  103.0 0.6 constant_dynamic-update-slice_fusion
  103.6 1.4 collective-permute-start.16
  105.1 0.6 collective-permute-start.17
  105.7 4.7 %collective-permute-done.16 = bf16[48,2176]{1,0:T(8,128)(2,1)S(1)} collective-permute-done((bf16[48,2176]{1,0:T(8,128)(2,1)S(1)}, bf16[48,2176]{1,0:T(8,128)(2,1)S(1)}, u32[]{:S(2)}, u32[]{:S(2)}) %collective-permute-start.16) | collective-permute-done | bytes 208928 | tf_op jit(solution)/shard_map/ppermute | solution.py:96
  110.4 1.7 collective-permute-start.18
  112.4 0.7 constant_dynamic-update-slice_fusion.7
  113.1 0.7 constant_dynamic-update-slice_fusion.6
  113.9 8.0 %collective-permute-done.18 = bf16[48,2176]{1,0:T(8,128)(2,1)S(1)} collective-permute-done((bf16[48,2176]{1,0:T(8,128)(2,1)S(1)}, bf16[48,2176]{1,0:T(8,128)(2,1)S(1)}, u32[]{:S(2)}, u32[]{:S(2)}) %collective-permute-start.18) | collective-permute-done | bytes 208928 | tf_op jit(solution)/shard_map/ppermute | solution.py:96
  121.8 2.7 collective-permute-start.20
  124.5 0.7 constant_dynamic-update-slice_fusion.5
  125.2 0.7 constant_dynamic-update-slice_fusion.4
  125.9 10.9 %collective-permute-done.21 = bf16[48,2176]{1,0:T(8,128)(2,1)S(1)} collective-permute-done((bf16[48,2176]{1,0:T(8,128)(2,1)S(1)}, bf16[48,2176]{1,0:T(8,128)(2,1)S(1)}, u32[]{:S(2)}, u32[]{:S(2)}) %collective-permute-start.21) | collective-permute-done | bytes 208928 | tf_op jit(solution)/shard_map/ppermute | solution.py:96
  137.0 3.5 %collective-permute-start.22 = (bf16[48,1024]{1,0:T(8,128)(2,1)S(1)}, bf16[48,1024]{1,0:T(8,128)(2,1)S(1)}, u32[]{:S(2)}, u32[]{:S(2)}) collective-permute-start(bf16[48,1024]{1,0:T(8,128)(2,1)S(1)} %slice.151), channel_id=1, source_target_pairs={{0,2},{2,4},{4,6},{6,8},{8,10},{10,12},{12,14},{14,0},{1,3},{3,5},... | collective-permute-start | bytes 294920 | tf_op jit(solution)/shard_map/ppermute | solution.py:96
  140.5 0.7 constant_dynamic-update-slice_fusion.3
  141.2 0.7 constant_dynamic-update-slice_fusion.2
  141.9 3.0 %collective-permute-done.22 = bf16[48,1024]{1,0:T(8,128)(2,1)S(1)} collective-permute-done((bf16[48,1024]{1,0:T(8,128)(2,1)S(1)}, bf16[48,1024]{1,0:T(8,128)(2,1)S(1)}, u32[]{:S(2)}, u32[]{:S(2)}) %collective-permute-start.22) | collective-permute-done | bytes 98336 | tf_op jit(solution)/shard_map/ppermute | solution.py:96
  144.8 0.5 collective-permute-done.23
  145.4 0.7 maximum_dynamic-update-slice_fusion.rows_in
  146.1 9.4 %experts.2 = bf16[384,2048]{1,0:T(8,128)(2,1)} custom-call(bf16[384,2176]{1,0:T(8,128)(2,1)} %maximum_dynamic-update-slice_fusion.rows_in, bf16[3,2048,128]{2,1,0:T(8,128)(2,1)} %refs_0_.1, bf16[3,2048,128]{2,1,0:T(8,128)(2,1)} %collective-permute-done.13.refs_1_, bf16[3,2048,128]{2,1,0:T(8,128)(2,1)} %refs_2_.1, ...), custom_call_target="tpu_custom_call" | custom-call | flops 3623878656 | bytes 20971520 | tf_op jit(solution)/shard_map/experts/pallas_call | solution.py:224
  155.5 5.5 %all-gather.2.cloned.1.call-done.rows_in = bf16[896,2176]{1,0:T(8,128)(2,1)} async-done(((bf16[112,2176]{1,0:T(8,128)(2,1)}), bf16[896,2176]{1,0:T(8,128)(2,1)}) %all-gather.2.cloned.1.call-update) | async-done | bytes 3899408 | tf_op jit(solution)/shard_map/all_gather | solution.py:339
  161.0 15.7 %experts.3 = bf16[896,2048]{1,0:T(8,128)(2,1)} custom-call(bf16[896,2176]{1,0:T(8,128)(2,1)} %all-gather.2.cloned.1.call-done.rows_in, bf16[3,2048,128]{2,1,0:T(8,128)(2,1)} %refs_0_.1, bf16[3,2048,128]{2,1,0:T(8,128)(2,1)} %collective-permute-done.13.refs_1_, bf16[3,2048,128]{2,1,0:T(8,128)(2,1)} %refs_2_.1, ...), custom_call_target="tpu_custom_call" | custom-call | flops 8455716864 | bytes 20971520 | tf_op jit(solution)/shard_map/experts/pallas_call | solution.py:224
  176.8 1.0 slice.130
  177.8 4.6 %collective-permute-done.24 = bf16[48,1024]{1,0:T(8,128)(2,1)S(1)} collective-permute-done((bf16[48,1024]{1,0:T(8,128)(2,1)S(1)}, bf16[48,1024]{1,0:T(8,128)(2,1)S(1)}, u32[]{:S(2)}, u32[]{:S(2)}) %collective-permute-start.24) | collective-permute-done | bytes 98336 | tf_op jit(solution)/shard_map/ppermute | solution.py:96
  182.4 1.1 slice_add_fusion.7
  183.6 3.3 %collective-permute-start.25 = (bf16[48,2048]{1,0:T(8,128)(2,1)S(1)}, bf16[48,2048]{1,0:T(8,128)(2,1)S(1)}, u32[]{:S(2)}, u32[]{:S(2)}) collective-permute-start(bf16[48,2048]{1,0:T(8,128)(2,1)S(1)} %pad_maximum_fusion.7), channel_id=1, source_target_pairs={{0,2},{2,4},{4,6},{6,8},{8,10},{10,12},{12,14},{14,0},{1,3},{3,5},... | collective-permute-start | bytes 589832 | tf_op jit(solution)/shard_map/ppermute | solution.py:96
  186.9 4.3 %collective-permute-done.28 = bf16[48,1024]{1,0:T(8,128)(2,1)S(1)} collective-permute-done((bf16[48,1024]{1,0:T(8,128)(2,1)S(1)}, bf16[48,1024]{1,0:T(8,128)(2,1)S(1)}, u32[]{:S(2)}, u32[]{:S(2)}) %collective-permute-start.28) | collective-permute-done | bytes 98336 | tf_op jit(solution)/shard_map/ppermute | solution.py:96
  191.2 0.9 slice_add_fusion.6
  192.2 3.3 %collective-permute-done.25 = bf16[48,2048]{1,0:T(8,128)(2,1)S(1)} collective-permute-done((bf16[48,2048]{1,0:T(8,128)(2,1)S(1)}, bf16[48,2048]{1,0:T(8,128)(2,1)S(1)}, u32[]{:S(2)}, u32[]{:S(2)}) %collective-permute-start.25) | collective-permute-done | bytes 196640 | tf_op jit(solution)/shard_map/ppermute | solution.py:96
  195.5 3.8 %collective-permute-start.26 = (bf16[48,2048]{1,0:T(8,128)(2,1)S(1)}, bf16[48,2048]{1,0:T(8,128)(2,1)S(1)}, u32[]{:S(2)}, u32[]{:S(2)}) collective-permute-start(bf16[48,2048]{1,0:T(8,128)(2,1)S(1)} %slice_add_fusion.2), channel_id=1, source_target_pairs={{0,2},{2,4},{4,6},{6,8},{8,10},{10,12},{12,14},{14,0},{1,3},{3,5},... | collective-permute-start | bytes 589832 | tf_op jit(solution)/shard_map/ppermute | solution.py:96
  199.3 4.4 %collective-permute-done.29 = bf16[48,2048]{1,0:T(8,128)(2,1)S(1)} collective-permute-done((bf16[48,2048]{1,0:T(8,128)(2,1)S(1)}, bf16[48,2048]{1,0:T(8,128)(2,1)S(1)}, u32[]{:S(2)}, u32[]{:S(2)}) %collective-permute-start.29) | collective-permute-done | bytes 196640 | tf_op jit(solution)/shard_map/ppermute | solution.py:96
  203.7 4.0 %collective-permute-done.26 = bf16[48,2048]{1,0:T(8,128)(2,1)S(1)} collective-permute-done((bf16[48,2048]{1,0:T(8,128)(2,1)S(1)}, bf16[48,2048]{1,0:T(8,128)(2,1)S(1)}, u32[]{:S(2)}, u32[]{:S(2)}) %collective-permute-start.26) | collective-permute-done | bytes 196640 | tf_op jit(solution)/shard_map/ppermute | solution.py:96
  207.8 3.8 %collective-permute-start.27 = (bf16[48,2048]{1,0:T(8,128)(2,1)S(1)}, bf16[48,2048]{1,0:T(8,128)(2,1)S(1)}, u32[]{:S(2)}, u32[]{:S(2)}) collective-permute-start(bf16[48,2048]{1,0:T(8,128)(2,1)S(1)} %get-tuple-element.25), channel_id=1, source_target_pairs={{0,2},{2,4},{4,6},{6,8},{8,10},{10,12},{12,14},{14,0},{1,3},{3,5},... | collective-permute-start | bytes 589832 | tf_op jit(solution)/shard_map/ppermute | solution.py:96
  211.6 8.2 %collective-permute-done.30 = bf16[48,2048]{1,0:T(8,128)(2,1)S(1)} collective-permute-done((bf16[48,2048]{1,0:T(8,128)(2,1)S(1)}, bf16[48,2048]{1,0:T(8,128)(2,1)S(1)}, u32[]{:S(2)}, u32[]{:S(2)}) %collective-permute-start.30) | collective-permute-done | bytes 196640 | tf_op jit(solution)/shard_map/ppermute | solution.py:96
  220.0 11.5 %collective-permute-done.31 = bf16[48,2048]{1,0:T(8,128)(2,1)S(1)} collective-permute-done((bf16[48,2048]{1,0:T(8,128)(2,1)S(1)}, bf16[48,2048]{1,0:T(8,128)(2,1)S(1)}, u32[]{:S(2)}, u32[]{:S(2)}) %collective-permute-start.31) | collective-permute-done | bytes 196640 | tf_op jit(solution)/shard_map/ppermute | solution.py:96
  231.5 0.8 reshape.167
  232.3 5.1 %all-to-all-start.2 = ((bf16[16,48,128]{2,1,0:T(8,128)(2,1)}), bf16[16,48,128]{2,1,0:T(8,128)(2,1)S(1)}, u32[]{:S(2)}, u32[]{:S(2)}) async-start(bf16[16,48,128]{2,1,0:T(8,128)(2,1)} %reshape.167), calls=%async_computation.4 | async-start | bytes 393216 | tf_op jit(solution)/shard_map/all_to_all | solution.py:325
  237.5 1.2 reshape.166
  238.8 7.0 %all-to-all-done.2 = bf16[16,48,128]{2,1,0:T(8,128)(2,1)S(1)} async-done(((bf16[16,48,128]{2,1,0:T(8,128)(2,1)}), bf16[16,48,128]{2,1,0:T(8,128)(2,1)S(1)}, u32[]{:S(2)}, u32[]{:S(2)}) %all-to-all-start.2) | async-done | bytes 196640 | tf_op jit(solution)/shard_map/all_to_all | solution.py:325
  245.7 12.7 %all_to_all.16 = bf16[16,112,128]{2,1,0:T(8,128)(2,1)S(1)} all-to-all(bf16[16,112,128]{2,1,0:T(8,128)(2,1)S(1)} %reshape.166), channel_id=1, replica_groups=mesh['sp'=16,'tp_0'=8,'tp_1'=2] {'sp'}, dimensions={0} | all-to-all | bytes 917504 | tf_op jit(solution)/shard_map/all_to_all | solution.py:325
  258.8 1.1 fusion.1
  (115 shorter events, 7.6 us)
Async XLA Ops:
  6.5 72.5 %reduce-scatter.3.cloned.1.call-start = ((), (), s32[]{:S(2)}) async-start(), calls=%async_computation.5 | async-start | bytes 2949120 | tf_op jit(solution)/shard_map/reduce_scatter | solution.py:309
  6.5 7.3 %copy-start.2 = (bf16[2048,128]{1,0:T(8,128)(2,1)S(1)}, bf16[2048,128]{1,0:T(8,128)(2,1)}, u32[]{:S(2)}) copy-start(bf16[2048,128]{1,0:T(8,128)(2,1)} %param.14) | copy-start | bytes 1572868
  6.5 7.9 %copy-start = (bf16[128,2048]{1,0:T(8,128)(2,1)S(1)}, bf16[128,2048]{1,0:T(8,128)(2,1)}, u32[]{:S(2)}) copy-start(bf16[128,2048]{1,0:T(8,128)(2,1)} %param.18) | copy-start | bytes 1572868
  7.9 8.9 %collective-permute-start.2 = (bf16[2,128,128]{2,1,0:T(8,128)(2,1)S(1)}, bf16[2,128,128]{2,1,0:T(8,128)(2,1)S(1)}, u32[]{:S(2)}, u32[]{:S(2)}) collective-permute-start(bf16[2,128,128]{2,1,0:T(8,128)(2,1)S(1)} %get-tuple-element.40), channel_id=1, source_target_pairs={{16,0},{32,16},{48,32},{64,48},{80,64},{96,80},{112,96},{128,112},... | collective-permute-start | bytes 196616 | tf_op jit(solution)/shard_map/ppermute | solution.py:33
  9.2 7.6 %collective-permute-start.1 = (bf16[2,128,128]{2,1,0:T(8,128)(2,1)S(1)}, bf16[2,128,128]{2,1,0:T(8,128)(2,1)S(1)}, u32[]{:S(2)}, u32[]{:S(2)}) collective-permute-start(bf16[2,128,128]{2,1,0:T(8,128)(2,1)S(1)} %get-tuple-element.39), channel_id=1, source_target_pairs={{0,16},{16,32},{32,48},{48,64},{64,80},{80,96},{96,112},{112,128},... | collective-permute-start | bytes 196616 | tf_op jit(solution)/shard_map/ppermute | solution.py:32
  13.9 3.6 %collective-permute-start = (bf16[8,1,128,128]{3,2,1,0:T(8,128)(2,1)S(1)}, bf16[8,1,128,128]{3,2,1,0:T(8,128)(2,1)S(1)}, u32[]{:S(2)}, u32[]{:S(2)}) collective-permute-start(bf16[8,1,128,128]{3,2,1,0:T(8,128)(2,1)S(1)} %get-tuple-element.42), channel_id=1, source_target_pairs={{0,1},{1,0},{2,3},{3,2},{4,5},{5,4},{6,7},{7,6},{8,9},{9,8},{10,11... | collective-permute-start | bytes 786440 | tf_op jit(solution)/shard_map/ppermute | solution.py:46
  14.0 2.1 collective-permute-start.3
  14.5 6.6 %collective-permute-start.4 = (bf16[128,2048]{1,0:T(8,128)(2,1)S(1)}, bf16[128,2048]{1,0:T(8,128)(2,1)S(1)}, u32[]{:S(2)}, u32[]{:S(2)}) collective-permute-start(bf16[128,2048]{1,0:T(8,128)(2,1)S(1)} %copy-done), channel_id=1, source_target_pairs={{0,1},{1,0},{2,3},{3,2},{4,5},{5,4},{6,7},{7,6},{8,9},{9,8},{10,11... | collective-permute-start | bytes 1572872 | tf_op jit(solution)/shard_map/ppermute | solution.py:299
  23.5 137.5 %all-gather.2.cloned.1.call-start = ((), (), s32[]{:S(2)}) async-start(), calls=%async_computation.6 | async-start | bytes 4386816 | tf_op jit(solution)/shard_map/all_gather | solution.py:339
  23.5 56.6 %collective-permute-start.13 = (bf16[3,2048,128]{2,1,0:T(8,128)(2,1)}, bf16[3,2048,128]{2,1,0:T(8,128)(2,1)}, u32[]{:S(2)}, u32[]{:S(2)}) collective-permute-start(bf16[3,2048,128]{2,1,0:T(8,128)(2,1)} %refs_0_.1), channel_id=1, source_target_pairs={{0,1},{1,0},{2,3},{3,2},{4,5},{5,4},{6,7},{7,6},{8,9},{9,8},{10,11... | collective-permute-start | bytes 4718600 | tf_op jit(solution)/shard_map/ppermute | solution.py:273
  24.0 56.1 %collective-permute-start.14 = (bf16[3,2048,128]{2,1,0:T(8,128)(2,1)}, bf16[3,2048,128]{2,1,0:T(8,128)(2,1)}, u32[]{:S(2)}, u32[]{:S(2)}) collective-permute-start(bf16[3,2048,128]{2,1,0:T(8,128)(2,1)} %refs_2_.1), channel_id=1, source_target_pairs={{0,1},{1,0},{2,3},{3,2},{4,5},{5,4},{6,7},{7,6},{8,9},{9,8},{10,11... | collective-permute-start | bytes 4718600 | tf_op jit(solution)/shard_map/ppermute | solution.py:273
  24.1 56.0 %collective-permute-start.15 = (bf16[3,128,2048]{2,1,0:T(8,128)(2,1)}, bf16[3,128,2048]{2,1,0:T(8,128)(2,1)}, u32[]{:S(2)}, u32[]{:S(2)}) collective-permute-start(bf16[3,128,2048]{2,1,0:T(8,128)(2,1)} %refs_4_.1), channel_id=1, source_target_pairs={{0,1},{1,0},{2,3},{3,2},{4,5},{5,4},{6,7},{7,6},{8,9},{9,8},{10,11... | collective-permute-start | bytes 4718600 | tf_op jit(solution)/shard_map/ppermute | solution.py:273
  24.5 3.9 %copy-start.6 = (s32[128]{0:T(128)S(1)}, s32[128]{0:T(128)}, u32[]{:S(2)}) copy-start(s32[128]{0:T(128)} %param.22) | copy-start | bytes 1540
  24.5 4.0 %copy-start.8 = (bf16[128,2]{0,1:T(2,128)(2,1)S(1)}, bf16[128,2]{0,1:T(2,128)(2,1)}, u32[]{:S(2)}) copy-start(bf16[128,2]{0,1:T(2,128)(2,1)} %param.24) | copy-start | bytes 1540
  25.2 16.8 %copy-start.7 = (s32[128,2]{0,1:T(2,128)S(1)}, s32[128,2]{0,1:T(2,128)}, u32[]{:S(2)}) copy-start(s32[128,2]{0,1:T(2,128)} %param.23) | copy-start | bytes 3076
  25.2 5.5 %collective-permute-start.5 = (bf16[128,384]{1,0:T(8,128)(2,1)S(1)}, bf16[128,384]{1,0:T(8,128)(2,1)S(1)}, u32[]{:S(2)}, u32[]{:S(2)}) collective-permute-start(bf16[128,384]{1,0:T(8,128)(2,1)S(1)} %get-tuple-element.47), channel_id=1, source_target_pairs={{0,2},{2,4},{4,6},{6,8},{8,10},{10,12},{12,14},{14,0},{1,3},{3,5},... | collective-permute-start | bytes 294920 | tf_op jit(solution)/shard_map/ppermute | solution.py:96
  28.5 6.0 %collective-permute-start.9 = (bf16[128,384]{1,0:T(8,128)(2,1)S(1)}, bf16[128,384]{1,0:T(8,128)(2,1)S(1)}, u32[]{:S(2)}, u32[]{:S(2)}) collective-permute-start(bf16[128,384]{1,0:T(8,128)(2,1)S(1)} %get-tuple-element.48), channel_id=1, source_target_pairs={{0,14},{2,0},{4,2},{6,4},{8,6},{10,8},{12,10},{14,12},{1,15},{3,1}... | collective-permute-start | bytes 294920 | tf_op jit(solution)/shard_map/ppermute | solution.py:96
  30.8 7.4 %collective-permute-start.6 = (bf16[128,768]{1,0:T(8,128)(2,1)S(1)}, bf16[128,768]{1,0:T(8,128)(2,1)S(1)}, u32[]{:S(2)}, u32[]{:S(2)}) collective-permute-start(bf16[128,768]{1,0:T(8,128)(2,1)S(1)} %pad_maximum_fusion.5), channel_id=1, source_target_pairs={{0,2},{2,4},{4,6},{6,8},{8,10},{10,12},{12,14},{14,0},{1,3},{3,5},... | collective-permute-start | bytes 589832 | tf_op jit(solution)/shard_map/ppermute | solution.py:96
  34.6 7.8 %collective-permute-start.10 = (bf16[128,768]{1,0:T(8,128)(2,1)S(1)}, bf16[128,768]{1,0:T(8,128)(2,1)S(1)}, u32[]{:S(2)}, u32[]{:S(2)}) collective-permute-start(bf16[128,768]{1,0:T(8,128)(2,1)S(1)} %pad_maximum_fusion.6), channel_id=1, source_target_pairs={{0,14},{2,0},{4,2},{6,4},{8,6},{10,8},{12,10},{14,12},{1,15},{3,1}... | collective-permute-start | bytes 589832 | tf_op jit(solution)/shard_map/ppermute | solution.py:96
  38.2 11.6 %collective-permute-start.7 = (bf16[128,768]{1,0:T(8,128)(2,1)S(1)}, bf16[128,768]{1,0:T(8,128)(2,1)S(1)}, u32[]{:S(2)}, u32[]{:S(2)}) collective-permute-start(bf16[128,768]{1,0:T(8,128)(2,1)S(1)} %bitcast_add_fusion.2), channel_id=1, source_target_pairs={{0,2},{2,4},{4,6},{6,8},{8,10},{10,12},{12,14},{14,0},{1,3},{3,5},... | collective-permute-start | bytes 589832 | tf_op jit(solution)/shard_map/ppermute | solution.py:96
  49.8 12.3 %collective-permute-start.11 = (bf16[128,768]{1,0:T(8,128)(2,1)S(1)}, bf16[128,768]{1,0:T(8,128)(2,1)S(1)}, u32[]{:S(2)}, u32[]{:S(2)}) collective-permute-start(bf16[128,768]{1,0:T(8,128)(2,1)S(1)} %get-tuple-element.32), channel_id=1, source_target_pairs={{0,14},{2,0},{4,2},{6,4},{8,6},{10,8},{12,10},{14,12},{1,15},{3,1}... | collective-permute-start | bytes 589832 | tf_op jit(solution)/shard_map/ppermute | solution.py:96
  49.9 12.6 %collective-permute-start.8 = (bf16[128,768]{1,0:T(8,128)(2,1)S(1)}, bf16[128,768]{1,0:T(8,128)(2,1)S(1)}, u32[]{:S(2)}, u32[]{:S(2)}) collective-permute-start(bf16[128,768]{1,0:T(8,128)(2,1)S(1)} %get-tuple-element.31), channel_id=1, source_target_pairs={{0,2},{2,4},{4,6},{6,8},{8,10},{10,12},{12,14},{14,0},{1,3},{3,5},... | collective-permute-start | bytes 589832 | tf_op jit(solution)/shard_map/ppermute | solution.py:96
  62.2 11.6 %collective-permute-start.12 = (bf16[128,768]{1,0:T(8,128)(2,1)S(1)}, bf16[128,768]{1,0:T(8,128)(2,1)S(1)}, u32[]{:S(2)}, u32[]{:S(2)}) collective-permute-start(bf16[128,768]{1,0:T(8,128)(2,1)S(1)} %bitcast_add_fusion.1), channel_id=1, source_target_pairs={{0,14},{2,0},{4,2},{6,4},{8,6},{10,8},{12,10},{14,12},{1,15},{3,1}... | collective-permute-start | bytes 589832 | tf_op jit(solution)/shard_map/ppermute | solution.py:96
  62.5 17.9 %copy-start.3 = (bf16[128,2048]{1,0:T(8,128)(2,1)S(1)}, bf16[128,2048]{1,0:T(8,128)(2,1)}, u32[]{:S(2)}) copy-start(bf16[128,2048]{1,0:T(8,128)(2,1)} %param.19) | copy-start | bytes 1572868
  62.5 17.8 %copy-start.4 = (f32[2048]{0:T(1024)S(1)}, f32[2048]{0:T(1024)}, u32[]{:S(2)}) copy-start(f32[2048]{0:T(1024)} %param.20) | copy-start | bytes 24580
  80.1 0.7 copy-start.5
  102.1 135.5 %reduce-scatter.5.cloned.1.call-start = ((), (), s32[]{:S(2)}) async-start(), calls=%async_computation.7 | async-start | bytes 4128768 | tf_op jit(solution)/shard_map/reduce_scatter | solution.py:344
  103.6 6.8 %collective-permute-start.16 = (bf16[48,2176]{1,0:T(8,128)(2,1)S(1)}, bf16[48,2176]{1,0:T(8,128)(2,1)S(1)}, u32[]{:S(2)}, u32[]{:S(2)}) collective-permute-start(bf16[48,2176]{1,0:T(8,128)(2,1)S(1)} %get-tuple-element.51), channel_id=1, source_target_pairs={{0,2},{2,4},{4,6},{6,8},{8,10},{10,12},{12,14},{14,0},{1,3},{3,5},... | collective-permute-start | bytes 626696 | tf_op jit(solution)/shard_map/ppermute | solution.py:96
  105.1 7.0 %collective-permute-start.17 = (bf16[48,2176]{1,0:T(8,128)(2,1)S(1)}, bf16[48,2176]{1,0:T(8,128)(2,1)S(1)}, u32[]{:S(2)}, u32[]{:S(2)}) collective-permute-start(bf16[48,2176]{1,0:T(8,128)(2,1)S(1)} %get-tuple-element.51), channel_id=1, source_target_pairs={{0,14},{2,0},{4,2},{6,4},{8,6},{10,8},{12,10},{14,12},{1,15},{3,1}... | collective-permute-start | bytes 626696 | tf_op jit(solution)/shard_map/ppermute | solution.py:96
  110.4 11.4 %collective-permute-start.18 = (bf16[48,2176]{1,0:T(8,128)(2,1)S(1)}, bf16[48,2176]{1,0:T(8,128)(2,1)S(1)}, u32[]{:S(2)}, u32[]{:S(2)}) collective-permute-start(bf16[48,2176]{1,0:T(8,128)(2,1)S(1)} %collective-permute-done.16), channel_id=1, source_target_pairs={{0,2},{2,4},{4,6},{6,8},{8,10},{10,12},{12,14},{14,0},{1,3},{3,5},... | collective-permute-start | bytes 626696 | tf_op jit(solution)/shard_map/ppermute | solution.py:96
  112.1 12.4 %collective-permute-start.19 = (bf16[48,2176]{1,0:T(8,128)(2,1)S(1)}, bf16[48,2176]{1,0:T(8,128)(2,1)S(1)}, u32[]{:S(2)}, u32[]{:S(2)}) collective-permute-start(bf16[48,2176]{1,0:T(8,128)(2,1)S(1)} %collective-permute-done.17), channel_id=1, source_target_pairs={{0,14},{2,0},{4,2},{6,4},{8,6},{10,8},{12,10},{14,12},{1,15},{3,1}... | collective-permute-start | bytes 626696 | tf_op jit(solution)/shard_map/ppermute | solution.py:96
  121.8 15.1 %collective-permute-start.20 = (bf16[48,2176]{1,0:T(8,128)(2,1)S(1)}, bf16[48,2176]{1,0:T(8,128)(2,1)S(1)}, u32[]{:S(2)}, u32[]{:S(2)}) collective-permute-start(bf16[48,2176]{1,0:T(8,128)(2,1)S(1)} %collective-permute-done.18), channel_id=1, source_target_pairs={{0,2},{2,4},{4,6},{6,8},{8,10},{10,12},{12,14},{14,0},{1,3},{3,5},... | collective-permute-start | bytes 626696 | tf_op jit(solution)/shard_map/ppermute | solution.py:96
  124.5 12.3 %collective-permute-start.21 = (bf16[48,2176]{1,0:T(8,128)(2,1)S(1)}, bf16[48,2176]{1,0:T(8,128)(2,1)S(1)}, u32[]{:S(2)}, u32[]{:S(2)}) collective-permute-start(bf16[48,2176]{1,0:T(8,128)(2,1)S(1)} %collective-permute-done.19), channel_id=1, source_target_pairs={{0,14},{2,0},{4,2},{6,4},{8,6},{10,8},{12,10},{14,12},{1,15},{3,1}... | collective-permute-start | bytes 626696 | tf_op jit(solution)/shard_map/ppermute | solution.py:96
  136.8 8.5 %collective-permute-start.23 = (bf16[48,1152]{1,0:T(8,128)(2,1)S(1)}, bf16[48,1152]{1,0:T(8,128)(2,1)S(1)}, u32[]{:S(2)}, u32[]{:S(2)}) collective-permute-start(bf16[48,1152]{1,0:T(8,128)(2,1)S(1)} %slice.152), channel_id=1, source_target_pairs={{0,14},{2,0},{4,2},{6,4},{8,6},{10,8},{12,10},{14,12},{1,15},{3,1}... | collective-permute-start | bytes 331784 | tf_op jit(solution)/shard_map/ppermute | solution.py:96
  137.0 7.9 %collective-permute-start.22 = (bf16[48,1024]{1,0:T(8,128)(2,1)S(1)}, bf16[48,1024]{1,0:T(8,128)(2,1)S(1)}, u32[]{:S(2)}, u32[]{:S(2)}) collective-permute-start(bf16[48,1024]{1,0:T(8,128)(2,1)S(1)} %slice.151), channel_id=1, source_target_pairs={{0,2},{2,4},{4,6},{6,8},{8,10},{10,12},{12,14},{14,0},{1,3},{3,5},... | collective-permute-start | bytes 294920 | tf_op jit(solution)/shard_map/ppermute | solution.py:96
  176.8 18.7 %copy-start.1 = (bf16[384,2048]{1,0:T(8,128)(2,1)S(1)}, bf16[384,2048]{1,0:T(8,128)(2,1)}, u32[]{:S(2)}) copy-start(bf16[384,2048]{1,0:T(8,128)(2,1)} %experts.2) | copy-start | bytes 4718596
  177.8 4.6 %collective-permute-start.24 = (bf16[48,1024]{1,0:T(8,128)(2,1)S(1)}, bf16[48,1024]{1,0:T(8,128)(2,1)S(1)}, u32[]{:S(2)}, u32[]{:S(2)}) collective-permute-start(bf16[48,1024]{1,0:T(8,128)(2,1)S(1)} %slice.130), channel_id=1, source_target_pairs={{0,2},{2,4},{4,6},{6,8},{8,10},{10,12},{12,14},{14,0},{1,3},{3,5},... | collective-permute-start | bytes 294920 | tf_op jit(solution)/shard_map/ppermute | solution.py:96
  183.5 7.7 %collective-permute-start.28 = (bf16[48,1024]{1,0:T(8,128)(2,1)S(1)}, bf16[48,1024]{1,0:T(8,128)(2,1)S(1)}, u32[]{:S(2)}, u32[]{:S(2)}) collective-permute-start(bf16[48,1024]{1,0:T(8,128)(2,1)S(1)} %get-tuple-element.28), channel_id=1, source_target_pairs={{0,14},{2,0},{4,2},{6,4},{8,6},{10,8},{12,10},{14,12},{1,15},{3,1}... | collective-permute-start | bytes 294920 | tf_op jit(solution)/shard_map/ppermute | solution.py:96
  183.6 11.9 %collective-permute-start.25 = (bf16[48,2048]{1,0:T(8,128)(2,1)S(1)}, bf16[48,2048]{1,0:T(8,128)(2,1)S(1)}, u32[]{:S(2)}, u32[]{:S(2)}) collective-permute-start(bf16[48,2048]{1,0:T(8,128)(2,1)S(1)} %pad_maximum_fusion.7), channel_id=1, source_target_pairs={{0,2},{2,4},{4,6},{6,8},{8,10},{10,12},{12,14},{14,0},{1,3},{3,5},... | collective-permute-start | bytes 589832 | tf_op jit(solution)/shard_map/ppermute | solution.py:96
  192.1 11.6 %collective-permute-start.29 = (bf16[48,2048]{1,0:T(8,128)(2,1)S(1)}, bf16[48,2048]{1,0:T(8,128)(2,1)S(1)}, u32[]{:S(2)}, u32[]{:S(2)}) collective-permute-start(bf16[48,2048]{1,0:T(8,128)(2,1)S(1)} %pad_maximum_fusion.8), channel_id=1, source_target_pairs={{0,14},{2,0},{4,2},{6,4},{8,6},{10,8},{12,10},{14,12},{1,15},{3,1}... | collective-permute-start | bytes 589832 | tf_op jit(solution)/shard_map/ppermute | solution.py:96
  195.5 12.2 %collective-permute-start.26 = (bf16[48,2048]{1,0:T(8,128)(2,1)S(1)}, bf16[48,2048]{1,0:T(8,128)(2,1)S(1)}, u32[]{:S(2)}, u32[]{:S(2)}) collective-permute-start(bf16[48,2048]{1,0:T(8,128)(2,1)S(1)} %slice_add_fusion.2), channel_id=1, source_target_pairs={{0,2},{2,4},{4,6},{6,8},{8,10},{10,12},{12,14},{14,0},{1,3},{3,5},... | collective-permute-start | bytes 589832 | tf_op jit(solution)/shard_map/ppermute | solution.py:96
  207.8 12.1 %collective-permute-start.30 = (bf16[48,2048]{1,0:T(8,128)(2,1)S(1)}, bf16[48,2048]{1,0:T(8,128)(2,1)S(1)}, u32[]{:S(2)}, u32[]{:S(2)}) collective-permute-start(bf16[48,2048]{1,0:T(8,128)(2,1)S(1)} %get-tuple-element.26), channel_id=1, source_target_pairs={{0,14},{2,0},{4,2},{6,4},{8,6},{10,8},{12,10},{14,12},{1,15},{3,1}... | collective-permute-start | bytes 589832 | tf_op jit(solution)/shard_map/ppermute | solution.py:96
  207.8 12.1 %collective-permute-start.27 = (bf16[48,2048]{1,0:T(8,128)(2,1)S(1)}, bf16[48,2048]{1,0:T(8,128)(2,1)S(1)}, u32[]{:S(2)}, u32[]{:S(2)}) collective-permute-start(bf16[48,2048]{1,0:T(8,128)(2,1)S(1)} %get-tuple-element.25), channel_id=1, source_target_pairs={{0,2},{2,4},{4,6},{6,8},{8,10},{10,12},{12,14},{14,0},{1,3},{3,5},... | collective-permute-start | bytes 589832 | tf_op jit(solution)/shard_map/ppermute | solution.py:96
  219.9 11.6 %collective-permute-start.31 = (bf16[48,2048]{1,0:T(8,128)(2,1)S(1)}, bf16[48,2048]{1,0:T(8,128)(2,1)S(1)}, u32[]{:S(2)}, u32[]{:S(2)}) collective-permute-start(bf16[48,2048]{1,0:T(8,128)(2,1)S(1)} %slice_add_fusion.1), channel_id=1, source_target_pairs={{0,14},{2,0},{4,2},{6,4},{8,6},{10,8},{12,10},{14,12},{1,15},{3,1}... | collective-permute-start | bytes 589832 | tf_op jit(solution)/shard_map/ppermute | solution.py:96
  232.3 13.5 %all-to-all-start.2 = ((bf16[16,48,128]{2,1,0:T(8,128)(2,1)}), bf16[16,48,128]{2,1,0:T(8,128)(2,1)S(1)}, u32[]{:S(2)}, u32[]{:S(2)}) async-start(bf16[16,48,128]{2,1,0:T(8,128)(2,1)} %reshape.167), calls=%async_computation.4 | async-start | bytes 393216 | tf_op jit(solution)/shard_map/all_to_all | solution.py:325
Sparse Core Ops, SparseCore 0:
  23.6 55.3 reduce-scatter.2
  102.2 58.7 all-gather.1
  176.9 60.6 reduce-scatter.4

commit v3 on v2

--- a/solution.py
+++ b/solution.py
@@ -145,8 +145,12 @@
     def row_copy(i):
         return pltpu.make_async_copy(rows_in.at[span(i)], rows.at[span(i)], row_sems.at[i])
 
-    def out_copy(i):
-        return pltpu.make_async_copy(out.at[span(i)], out_to.at[span(i)], out_sems.at[i])
+    def columns(c):
+        return pl.ds(pl.multiple_of(c * wide, wide), wide)
+
+    def out_copy(i, c):
+        at = (span(i), columns(c))
+        return pltpu.make_async_copy(out.at[at], out_to.at[at], out_sems.at[i, c])
 
     row_copy(0).start()
     for k in range(4):
@@ -198,18 +202,18 @@
 
         @pl.loop(0, width // wide)
         def _(c):
-            cols = pl.ds(pl.multiple_of(c * wide, wide), wide)
+            cols = columns(c)
             pieces = []
             for e in range(GROUP_EXPERTS):
                 pieces += [down_own[e, :, cols], down_far[e, :, cols]]
             out[span(i), cols] = jnp.dot(
                 joined, jnp.concatenate(pieces, axis=0), preferred_element_type=jnp.float32
             ).astype(jnp.bfloat16)
-
-        out_copy(i).start()
+            out_copy(i, c).start()
 
     for i in range(steps):
-        out_copy(i).wait()
+        for c in range(width // wide):
+            out_copy(i, c).wait()
 
 
 def experts(rows, gate_pair, up_pair, down_pair):
@@ -234,7 +238,7 @@
             pltpu.VMEM((total, width), jnp.bfloat16),
             pltpu.SemaphoreType.DMA((6, GROUP_EXPERTS)),
             pltpu.SemaphoreType.DMA((steps,)),
-            pltpu.SemaphoreType.DMA((steps,)),
+            pltpu.SemaphoreType.DMA((steps, width // 512)),
         ],
         compiler_params=pltpu.CompilerParams(vmem_limit_bytes=62 * 2**20),
         cost_estimate=pl.CostEstimate(

time: 267 us -> 267 us (level)
  transfers between devices with their start and end apart: 36 -> 36, of which waited for: 21 -> 21; matrix products, arithmetic and copies ran while one was open for 7% -> 7% of each run, Pallas kernels for 4% -> 3%
where the time goes in v3:
time: 267 us; the launch traced here: 266 us
  waiting for transfers between devices  118 us (44%)
  starting transfers between devices  49.3 us (18%)
  blocking collectives  32.1 us (12%)
  Pallas kernels  24.5 us (9%)
  between operations  14.5 us (5%)
  local copies, waits for them, and re-layouts  11.6 us (4%)
  other arithmetic  9.21 us (3%)
  matrix products  6.82 us (3%)
    ppermute x12, waiting for transfers between devices, shifts(): lax.ppermute(a, Z, down)  59.7 us
    ppermute x12, waiting for transfers between devices, shifts(): lax.ppermute(a, Z, up)  40.2 us
    ppermute x12, starting transfers between devices, shifts(): lax.ppermute(a, Z, up)  34.7 us
    all_to_all x2, blocking collectives, exchange(): lax.all_to_all(rows.reshape(groups, -1, LANES), 'sp', split_axis=0, conca...  32.1 us
    pallas_call x2, Pallas kernels, experts(): pl.pallas_call(experts_kernel, in_specs=[anywhere] * 7, out_specs=anywher...  24.5 us
    all_to_all x1, waiting for transfers between devices, exchange(): lax.all_to_all(rows.reshape(groups, -1, LANES), 'sp', split_axis=0, conca...  6.94 us
    all_gather x1, waiting for transfers between devices, per_device(): pool_a = lax.all_gather(with_gates(0, cap_a), Z, axis=0, tiled=True)  5.84 us
  transfers between devices with their start and end apart: 36, of which 21 were waited for; matrix products, arithmetic and copies ran while one was open for 7% of the time, Pallas kernels for 3%

profile of v3, /device:TPU:96, one launch (start us, length us, event | category | flops | bytes accessed | tf_op | source)
XLA Modules:
  0.0 266.2 jit_solution(9399889828197799947)
XLA Ops:
  6.5 1.4 dynamic-slice_bitcast_fusion
  7.9 1.3 collective-permute-start.2
  9.2 4.5 %collective-permute-start.1 = (bf16[2,128,128]{2,1,0:T(8,128)(2,1)S(1)}, bf16[2,128,128]{2,1,0:T(8,128)(2,1)S(1)}, u32[]{:S(2)}, u32[]{:S(2)}) collective-permute-start(bf16[2,128,128]{2,1,0:T(8,128)(2,1)S(1)} %get-tuple-element.39), channel_id=1, source_target_pairs={{0,16},{16,32},{32,48},{48,64},{64,80},{80,96},{96,112},{112,128},... | collective-permute-start | bytes 196616 | tf_op jit(solution)/shard_map/ppermute | solution.py:32
  15.4 0.6 fusion.4
  16.1 0.7 pad_maximum_fusion.11
  17.4 0.9 fusion
  18.4 1.3 fusion.2
  19.7 1.3 fusion.7
  21.1 2.3 bitcast_convert_fusion
  24.5 0.6 bitcast_convert_fusion.1
  25.2 3.2 %collective-permute-start.5 = (bf16[128,384]{1,0:T(8,128)(2,1)S(1)}, bf16[128,384]{1,0:T(8,128)(2,1)S(1)}, u32[]{:S(2)}, u32[]{:S(2)}) collective-permute-start(bf16[128,384]{1,0:T(8,128)(2,1)S(1)} %get-tuple-element.47), channel_id=1, source_target_pairs={{0,2},{2,4},{4,6},{6,8},{8,10},{10,12},{12,14},{14,0},{1,3},{3,5},... | collective-permute-start | bytes 294920 | tf_op jit(solution)/shard_map/ppermute | solution.py:96
  28.6 2.1 collective-permute-done.5
  30.8 3.8 %collective-permute-start.6 = (bf16[128,768]{1,0:T(8,128)(2,1)S(1)}, bf16[128,768]{1,0:T(8,128)(2,1)S(1)}, u32[]{:S(2)}, u32[]{:S(2)}) collective-permute-start(bf16[128,768]{1,0:T(8,128)(2,1)S(1)} %pad_maximum_fusion.5), channel_id=1, source_target_pairs={{0,2},{2,4},{4,6},{6,8},{8,10},{10,12},{12,14},{14,0},{1,3},{3,5},... | collective-permute-start | bytes 589832 | tf_op jit(solution)/shard_map/ppermute | solution.py:96
  34.9 3.3 %collective-permute-done.6 = bf16[128,768]{1,0:T(8,128)(2,1)S(1)} collective-permute-done((bf16[128,768]{1,0:T(8,128)(2,1)S(1)}, bf16[128,768]{1,0:T(8,128)(2,1)S(1)}, u32[]{:S(2)}, u32[]{:S(2)}) %collective-permute-start.6) | collective-permute-done | bytes 196640 | tf_op jit(solution)/shard_map/ppermute | solution.py:96
  38.2 3.8 %collective-permute-start.7 = (bf16[128,768]{1,0:T(8,128)(2,1)S(1)}, bf16[128,768]{1,0:T(8,128)(2,1)S(1)}, u32[]{:S(2)}, u32[]{:S(2)}) collective-permute-start(bf16[128,768]{1,0:T(8,128)(2,1)S(1)} %bitcast_add_fusion.2), channel_id=1, source_target_pairs={{0,2},{2,4},{4,6},{6,8},{8,10},{10,12},{12,14},{14,0},{1,3},{3,5},... | collective-permute-start | bytes 589832 | tf_op jit(solution)/shard_map/ppermute | solution.py:96
  42.4 7.4 %collective-permute-done.7 = bf16[128,768]{1,0:T(8,128)(2,1)S(1)} collective-permute-done((bf16[128,768]{1,0:T(8,128)(2,1)S(1)}, bf16[128,768]{1,0:T(8,128)(2,1)S(1)}, u32[]{:S(2)}, u32[]{:S(2)}) %collective-permute-start.7) | collective-permute-done | bytes 196640 | tf_op jit(solution)/shard_map/ppermute | solution.py:96
  49.9 3.8 %collective-permute-start.8 = (bf16[128,768]{1,0:T(8,128)(2,1)S(1)}, bf16[128,768]{1,0:T(8,128)(2,1)S(1)}, u32[]{:S(2)}, u32[]{:S(2)}) collective-permute-start(bf16[128,768]{1,0:T(8,128)(2,1)S(1)} %get-tuple-element.31), channel_id=1, source_target_pairs={{0,2},{2,4},{4,6},{6,8},{8,10},{10,12},{12,14},{14,0},{1,3},{3,5},... | collective-permute-start | bytes 589832 | tf_op jit(solution)/shard_map/ppermute | solution.py:96
  53.7 8.5 %collective-permute-done.11 = bf16[128,768]{1,0:T(8,128)(2,1)S(1)} collective-permute-done((bf16[128,768]{1,0:T(8,128)(2,1)S(1)}, bf16[128,768]{1,0:T(8,128)(2,1)S(1)}, u32[]{:S(2)}, u32[]{:S(2)}) %collective-permute-start.11) | collective-permute-done | bytes 196640 | tf_op jit(solution)/shard_map/ppermute | solution.py:96
  62.5 11.3 %collective-permute-done.12 = bf16[128,768]{1,0:T(8,128)(2,1)S(1)} collective-permute-done((bf16[128,768]{1,0:T(8,128)(2,1)S(1)}, bf16[128,768]{1,0:T(8,128)(2,1)S(1)}, u32[]{:S(2)}, u32[]{:S(2)}) %collective-permute-start.12) | collective-permute-done | bytes 196640 | tf_op jit(solution)/shard_map/ppermute | solution.py:96
  73.8 5.2 %reduce-scatter.3.cloned.1.call-done = bf16[128,1280]{1,0:T(8,128)(2,1)} async-done(((bf16[1024,1280]{1,0:T(8,128)(2,1)}), bf16[128,1280]{1,0:T(8,128)(2,1)}) %reduce-scatter.3.cloned.1.call-update) | async-done | bytes 327696 | tf_op jit(solution)/shard_map/reduce_scatter | solution.py:313
  79.0 1.1 maximum_convert_fusion
  81.6 19.4 %all_to_all.15 = bf16[16,176,128]{2,1,0:T(8,128)(2,1)S(1)} all-to-all(bf16[16,176,128]{2,1,0:T(8,128)(2,1)S(1)} %fusion.12), channel_id=1, replica_groups=mesh['sp'=16,'tp_0'=8,'tp_1'=2] {'sp'}, dimensions={0} | all-to-all | bytes 1441792 | tf_op jit(solution)/shard_map/all_to_all | solution.py:329
  101.2 0.8 pad_maximum_fusion.3
  102.3 0.7 constant_dynamic-update-slice_fusion.1
  103.0 0.6 constant_dynamic-update-slice_fusion
  103.6 1.4 collective-permute-start.16
  105.1 0.6 collective-permute-start.17
  105.7 4.7 %collective-permute-done.16 = bf16[48,2176]{1,0:T(8,128)(2,1)S(1)} collective-permute-done((bf16[48,2176]{1,0:T(8,128)(2,1)S(1)}, bf16[48,2176]{1,0:T(8,128)(2,1)S(1)}, u32[]{:S(2)}, u32[]{:S(2)}) %collective-permute-start.16) | collective-permute-done | bytes 208928 | tf_op jit(solution)/shard_map/ppermute | solution.py:96
  110.4 1.7 collective-permute-start.18
  112.4 0.7 constant_dynamic-update-slice_fusion.7
  113.1 0.7 constant_dynamic-update-slice_fusion.6
  113.9 8.0 %collective-permute-done.18 = bf16[48,2176]{1,0:T(8,128)(2,1)S(1)} collective-permute-done((bf16[48,2176]{1,0:T(8,128)(2,1)S(1)}, bf16[48,2176]{1,0:T(8,128)(2,1)S(1)}, u32[]{:S(2)}, u32[]{:S(2)}) %collective-permute-start.18) | collective-permute-done | bytes 208928 | tf_op jit(solution)/shard_map/ppermute | solution.py:96
  121.8 2.7 %collective-permute-start.20 = (bf16[48,2176]{1,0:T(8,128)(2,1)S(1)}, bf16[48,2176]{1,0:T(8,128)(2,1)S(1)}, u32[]{:S(2)}, u32[]{:S(2)}) collective-permute-start(bf16[48,2176]{1,0:T(8,128)(2,1)S(1)} %collective-permute-done.18), channel_id=1, source_target_pairs={{0,2},{2,4},{4,6},{6,8},{8,10},{10,12},{12,14},{14,0},{1,3},{3,5},... | collective-permute-start | bytes 626696 | tf_op jit(solution)/shard_map/ppermute | solution.py:96
  124.5 0.7 constant_dynamic-update-slice_fusion.5
  125.2 0.7 constant_dynamic-update-slice_fusion.4
  125.9 10.9 %collective-permute-done.21 = bf16[48,2176]{1,0:T(8,128)(2,1)S(1)} collective-permute-done((bf16[48,2176]{1,0:T(8,128)(2,1)S(1)}, bf16[48,2176]{1,0:T(8,128)(2,1)S(1)}, u32[]{:S(2)}, u32[]{:S(2)}) %collective-permute-start.21) | collective-permute-done | bytes 208928 | tf_op jit(solution)/shard_map/ppermute | solution.py:96
  137.0 3.5 %collective-permute-start.22 = (bf16[48,1024]{1,0:T(8,128)(2,1)S(1)}, bf16[48,1024]{1,0:T(8,128)(2,1)S(1)}, u32[]{:S(2)}, u32[]{:S(2)}) collective-permute-start(bf16[48,1024]{1,0:T(8,128)(2,1)S(1)} %slice.151), channel_id=1, source_target_pairs={{0,2},{2,4},{4,6},{6,8},{8,10},{10,12},{12,14},{14,0},{1,3},{3,5},... | collective-permute-start | bytes 294920 | tf_op jit(solution)/shard_map/ppermute | solution.py:96
  140.5 0.7 constant_dynamic-update-slice_fusion.3
  141.2 0.7 constant_dynamic-update-slice_fusion.2
  141.9 3.0 %collective-permute-done.22 = bf16[48,1024]{1,0:T(8,128)(2,1)S(1)} collective-permute-done((bf16[48,1024]{1,0:T(8,128)(2,1)S(1)}, bf16[48,1024]{1,0:T(8,128)(2,1)S(1)}, u32[]{:S(2)}, u32[]{:S(2)}) %collective-permute-start.22) | collective-permute-done | bytes 98336 | tf_op jit(solution)/shard_map/ppermute | solution.py:96
  144.8 0.5 collective-permute-done.23
  145.4 0.7 maximum_dynamic-update-slice_fusion.rows_in
  146.1 9.0 %experts.2 = bf16[384,2048]{1,0:T(8,128)(2,1)} custom-call(bf16[384,2176]{1,0:T(8,128)(2,1)} %maximum_dynamic-update-slice_fusion.rows_in, bf16[3,2048,128]{2,1,0:T(8,128)(2,1)} %refs_0_.1, bf16[3,2048,128]{2,1,0:T(8,128)(2,1)} %collective-permute-done.13.refs_1_, bf16[3,2048,128]{2,1,0:T(8,128)(2,1)} %refs_2_.1, ...), custom_call_target="tpu_custom_call" | custom-call | flops 3623878656 | bytes 20971520 | tf_op jit(solution)/shard_map/experts/pallas_call | solution.py:228
  155.1 5.8 %all-gather.2.cloned.1.call-done.rows_in = bf16[896,2176]{1,0:T(8,128)(2,1)} async-done(((bf16[112,2176]{1,0:T(8,128)(2,1)}), bf16[896,2176]{1,0:T(8,128)(2,1)}) %all-gather.2.cloned.1.call-update) | async-done | bytes 3899408 | tf_op jit(solution)/shard_map/all_gather | solution.py:343
  161.0 15.5 %experts.3 = bf16[896,2048]{1,0:T(8,128)(2,1)} custom-call(bf16[896,2176]{1,0:T(8,128)(2,1)} %all-gather.2.cloned.1.call-done.rows_in, bf16[3,2048,128]{2,1,0:T(8,128)(2,1)} %refs_0_.1, bf16[3,2048,128]{2,1,0:T(8,128)(2,1)} %collective-permute-done.13.refs_1_, bf16[3,2048,128]{2,1,0:T(8,128)(2,1)} %refs_2_.1, ...), custom_call_target="tpu_custom_call" | custom-call | flops 8455716864 | bytes 20971520 | tf_op jit(solution)/shard_map/experts/pallas_call | solution.py:228
  176.5 1.0 slice.130
  177.6 4.6 %collective-permute-done.24 = bf16[48,1024]{1,0:T(8,128)(2,1)S(1)} collective-permute-done((bf16[48,1024]{1,0:T(8,128)(2,1)S(1)}, bf16[48,1024]{1,0:T(8,128)(2,1)S(1)}, u32[]{:S(2)}, u32[]{:S(2)}) %collective-permute-start.24) | collective-permute-done | bytes 98336 | tf_op jit(solution)/shard_map/ppermute | solution.py:96
  182.1 1.1 slice_add_fusion.7
  183.3 3.3 %collective-permute-start.25 = (bf16[48,2048]{1,0:T(8,128)(2,1)S(1)}, bf16[48,2048]{1,0:T(8,128)(2,1)S(1)}, u32[]{:S(2)}, u32[]{:S(2)}) collective-permute-start(bf16[48,2048]{1,0:T(8,128)(2,1)S(1)} %pad_maximum_fusion.7), channel_id=1, source_target_pairs={{0,2},{2,4},{4,6},{6,8},{8,10},{10,12},{12,14},{14,0},{1,3},{3,5},... | collective-permute-start | bytes 589832 | tf_op jit(solution)/shard_map/ppermute | solution.py:96
  186.6 4.3 %collective-permute-done.28 = bf16[48,1024]{1,0:T(8,128)(2,1)S(1)} collective-permute-done((bf16[48,1024]{1,0:T(8,128)(2,1)S(1)}, bf16[48,1024]{1,0:T(8,128)(2,1)S(1)}, u32[]{:S(2)}, u32[]{:S(2)}) %collective-permute-start.28) | collective-permute-done | bytes 98336 | tf_op jit(solution)/shard_map/ppermute | solution.py:96
  190.9 0.9 slice_add_fusion.6
  192.0 3.3 %collective-permute-done.25 = bf16[48,2048]{1,0:T(8,128)(2,1)S(1)} collective-permute-done((bf16[48,2048]{1,0:T(8,128)(2,1)S(1)}, bf16[48,2048]{1,0:T(8,128)(2,1)S(1)}, u32[]{:S(2)}, u32[]{:S(2)}) %collective-permute-start.25) | collective-permute-done | bytes 196640 | tf_op jit(solution)/shard_map/ppermute | solution.py:96
  195.3 3.8 %collective-permute-start.26 = (bf16[48,2048]{1,0:T(8,128)(2,1)S(1)}, bf16[48,2048]{1,0:T(8,128)(2,1)S(1)}, u32[]{:S(2)}, u32[]{:S(2)}) collective-permute-start(bf16[48,2048]{1,0:T(8,128)(2,1)S(1)} %slice_add_fusion.2), channel_id=1, source_target_pairs={{0,2},{2,4},{4,6},{6,8},{8,10},{10,12},{12,14},{14,0},{1,3},{3,5},... | collective-permute-start | bytes 589832 | tf_op jit(solution)/shard_map/ppermute | solution.py:96
  199.0 4.4 %collective-permute-done.29 = bf16[48,2048]{1,0:T(8,128)(2,1)S(1)} collective-permute-done((bf16[48,2048]{1,0:T(8,128)(2,1)S(1)}, bf16[48,2048]{1,0:T(8,128)(2,1)S(1)}, u32[]{:S(2)}, u32[]{:S(2)}) %collective-permute-start.29) | collective-permute-done | bytes 196640 | tf_op jit(solution)/shard_map/ppermute | solution.py:96
  203.4 4.0 %collective-permute-done.26 = bf16[48,2048]{1,0:T(8,128)(2,1)S(1)} collective-permute-done((bf16[48,2048]{1,0:T(8,128)(2,1)S(1)}, bf16[48,2048]{1,0:T(8,128)(2,1)S(1)}, u32[]{:S(2)}, u32[]{:S(2)}) %collective-permute-start.26) | collective-permute-done | bytes 196640 | tf_op jit(solution)/shard_map/ppermute | solution.py:96
  207.6 3.8 %collective-permute-start.27 = (bf16[48,2048]{1,0:T(8,128)(2,1)S(1)}, bf16[48,2048]{1,0:T(8,128)(2,1)S(1)}, u32[]{:S(2)}, u32[]{:S(2)}) collective-permute-start(bf16[48,2048]{1,0:T(8,128)(2,1)S(1)} %get-tuple-element.25), channel_id=1, source_target_pairs={{0,2},{2,4},{4,6},{6,8},{8,10},{10,12},{12,14},{14,0},{1,3},{3,5},... | collective-permute-start | bytes 589832 | tf_op jit(solution)/shard_map/ppermute | solution.py:96
  211.3 8.2 %collective-permute-done.30 = bf16[48,2048]{1,0:T(8,128)(2,1)S(1)} collective-permute-done((bf16[48,2048]{1,0:T(8,128)(2,1)S(1)}, bf16[48,2048]{1,0:T(8,128)(2,1)S(1)}, u32[]{:S(2)}, u32[]{:S(2)}) %collective-permute-start.30) | collective-permute-done | bytes 196640 | tf_op jit(solution)/shard_map/ppermute | solution.py:96
  219.7 11.5 %collective-permute-done.31 = bf16[48,2048]{1,0:T(8,128)(2,1)S(1)} collective-permute-done((bf16[48,2048]{1,0:T(8,128)(2,1)S(1)}, bf16[48,2048]{1,0:T(8,128)(2,1)S(1)}, u32[]{:S(2)}, u32[]{:S(2)}) %collective-permute-start.31) | collective-permute-done | bytes 196640 | tf_op jit(solution)/shard_map/ppermute | solution.py:96
  231.2 0.8 reshape.167
  232.0 5.1 %all-to-all-start.2 = ((bf16[16,48,128]{2,1,0:T(8,128)(2,1)}), bf16[16,48,128]{2,1,0:T(8,128)(2,1)S(1)}, u32[]{:S(2)}, u32[]{:S(2)}) async-start(bf16[16,48,128]{2,1,0:T(8,128)(2,1)} %reshape.167), calls=%async_computation.4 | async-start | bytes 393216 | tf_op jit(solution)/shard_map/all_to_all | solution.py:329
  237.3 1.2 reshape.166
  238.5 6.9 %all-to-all-done.2 = bf16[16,48,128]{2,1,0:T(8,128)(2,1)S(1)} async-done(((bf16[16,48,128]{2,1,0:T(8,128)(2,1)}), bf16[16,48,128]{2,1,0:T(8,128)(2,1)S(1)}, u32[]{:S(2)}, u32[]{:S(2)}) %all-to-all-start.2) | async-done | bytes 196640 | tf_op jit(solution)/shard_map/all_to_all | solution.py:329
  245.5 12.7 %all_to_all.16 = bf16[16,112,128]{2,1,0:T(8,128)(2,1)S(1)} all-to-all(bf16[16,112,128]{2,1,0:T(8,128)(2,1)S(1)} %reshape.166), channel_id=1, replica_groups=mesh['sp'=16,'tp_0'=8,'tp_1'=2] {'sp'}, dimensions={0} | all-to-all | bytes 917504 | tf_op jit(solution)/shard_map/all_to_all | solution.py:329
  258.5 1.1 fusion.1
  (115 shorter events, 7.6 us)
Async XLA Ops:
  6.5 72.5 %reduce-scatter.3.cloned.1.call-start = ((), (), s32[]{:S(2)}) async-start(), calls=%async_computation.5 | async-start | bytes 2949120 | tf_op jit(solution)/shard_map/reduce_scatter | solution.py:313
  6.5 7.3 %copy-start.2 = (bf16[2048,128]{1,0:T(8,128)(2,1)S(1)}, bf16[2048,128]{1,0:T(8,128)(2,1)}, u32[]{:S(2)}) copy-start(bf16[2048,128]{1,0:T(8,128)(2,1)} %param.14) | copy-start | bytes 1572868
  6.5 7.9 %copy-start = (bf16[128,2048]{1,0:T(8,128)(2,1)S(1)}, bf16[128,2048]{1,0:T(8,128)(2,1)}, u32[]{:S(2)}) copy-start(bf16[128,2048]{1,0:T(8,128)(2,1)} %param.18) | copy-start | bytes 1572868
  7.9 8.9 %collective-permute-start.2 = (bf16[2,128,128]{2,1,0:T(8,128)(2,1)S(1)}, bf16[2,128,128]{2,1,0:T(8,128)(2,1)S(1)}, u32[]{:S(2)}, u32[]{:S(2)}) collective-permute-start(bf16[2,128,128]{2,1,0:T(8,128)(2,1)S(1)} %get-tuple-element.40), channel_id=1, source_target_pairs={{16,0},{32,16},{48,32},{64,48},{80,64},{96,80},{112,96},{128,112},... | collective-permute-start | bytes 196616 | tf_op jit(solution)/shard_map/ppermute | solution.py:33
  9.2 7.6 %collective-permute-start.1 = (bf16[2,128,128]{2,1,0:T(8,128)(2,1)S(1)}, bf16[2,128,128]{2,1,0:T(8,128)(2,1)S(1)}, u32[]{:S(2)}, u32[]{:S(2)}) collective-permute-start(bf16[2,128,128]{2,1,0:T(8,128)(2,1)S(1)} %get-tuple-element.39), channel_id=1, source_target_pairs={{0,16},{16,32},{32,48},{48,64},{64,80},{80,96},{96,112},{112,128},... | collective-permute-start | bytes 196616 | tf_op jit(solution)/shard_map/ppermute | solution.py:32
  13.9 3.6 %collective-permute-start = (bf16[8,1,128,128]{3,2,1,0:T(8,128)(2,1)S(1)}, bf16[8,1,128,128]{3,2,1,0:T(8,128)(2,1)S(1)}, u32[]{:S(2)}, u32[]{:S(2)}) collective-permute-start(bf16[8,1,128,128]{3,2,1,0:T(8,128)(2,1)S(1)} %get-tuple-element.42), channel_id=1, source_target_pairs={{0,1},{1,0},{2,3},{3,2},{4,5},{5,4},{6,7},{7,6},{8,9},{9,8},{10,11... | collective-permute-start | bytes 786440 | tf_op jit(solution)/shard_map/ppermute | solution.py:46
  14.0 2.1 collective-permute-start.3
  14.5 6.6 %collective-permute-start.4 = (bf16[128,2048]{1,0:T(8,128)(2,1)S(1)}, bf16[128,2048]{1,0:T(8,128)(2,1)S(1)}, u32[]{:S(2)}, u32[]{:S(2)}) collective-permute-start(bf16[128,2048]{1,0:T(8,128)(2,1)S(1)} %copy-done), channel_id=1, source_target_pairs={{0,1},{1,0},{2,3},{3,2},{4,5},{5,4},{6,7},{7,6},{8,9},{9,8},{10,11... | collective-permute-start | bytes 1572872 | tf_op jit(solution)/shard_map/ppermute | solution.py:303
  23.5 137.5 %all-gather.2.cloned.1.call-start = ((), (), s32[]{:S(2)}) async-start(), calls=%async_computation.6 | async-start | bytes 4386816 | tf_op jit(solution)/shard_map/all_gather | solution.py:343
  23.5 56.6 %collective-permute-start.13 = (bf16[3,2048,128]{2,1,0:T(8,128)(2,1)}, bf16[3,2048,128]{2,1,0:T(8,128)(2,1)}, u32[]{:S(2)}, u32[]{:S(2)}) collective-permute-start(bf16[3,2048,128]{2,1,0:T(8,128)(2,1)} %refs_0_.1), channel_id=1, source_target_pairs={{0,1},{1,0},{2,3},{3,2},{4,5},{5,4},{6,7},{7,6},{8,9},{9,8},{10,11... | collective-permute-start | bytes 4718600 | tf_op jit(solution)/shard_map/ppermute | solution.py:277
  24.0 56.1 %collective-permute-start.14 = (bf16[3,2048,128]{2,1,0:T(8,128)(2,1)}, bf16[3,2048,128]{2,1,0:T(8,128)(2,1)}, u32[]{:S(2)}, u32[]{:S(2)}) collective-permute-start(bf16[3,2048,128]{2,1,0:T(8,128)(2,1)} %refs_2_.1), channel_id=1, source_target_pairs={{0,1},{1,0},{2,3},{3,2},{4,5},{5,4},{6,7},{7,6},{8,9},{9,8},{10,11... | collective-permute-start | bytes 4718600 | tf_op jit(solution)/shard_map/ppermute | solution.py:277
  24.1 56.0 %collective-permute-start.15 = (bf16[3,128,2048]{2,1,0:T(8,128)(2,1)}, bf16[3,128,2048]{2,1,0:T(8,128)(2,1)}, u32[]{:S(2)}, u32[]{:S(2)}) collective-permute-start(bf16[3,128,2048]{2,1,0:T(8,128)(2,1)} %refs_4_.1), channel_id=1, source_target_pairs={{0,1},{1,0},{2,3},{3,2},{4,5},{5,4},{6,7},{7,6},{8,9},{9,8},{10,11... | collective-permute-start | bytes 4718600 | tf_op jit(solution)/shard_map/ppermute | solution.py:277
  24.5 3.9 %copy-start.6 = (s32[128]{0:T(128)S(1)}, s32[128]{0:T(128)}, u32[]{:S(2)}) copy-start(s32[128]{0:T(128)} %param.22) | copy-start | bytes 1540
  24.5 4.0 %copy-start.8 = (bf16[128,2]{0,1:T(2,128)(2,1)S(1)}, bf16[128,2]{0,1:T(2,128)(2,1)}, u32[]{:S(2)}) copy-start(bf16[128,2]{0,1:T(2,128)(2,1)} %param.24) | copy-start | bytes 1540
  25.2 16.8 %copy-start.7 = (s32[128,2]{0,1:T(2,128)S(1)}, s32[128,2]{0,1:T(2,128)}, u32[]{:S(2)}) copy-start(s32[128,2]{0,1:T(2,128)} %param.23) | copy-start | bytes 3076
  25.2 5.5 %collective-permute-start.5 = (bf16[128,384]{1,0:T(8,128)(2,1)S(1)}, bf16[128,384]{1,0:T(8,128)(2,1)S(1)}, u32[]{:S(2)}, u32[]{:S(2)}) collective-permute-start(bf16[128,384]{1,0:T(8,128)(2,1)S(1)} %get-tuple-element.47), channel_id=1, source_target_pairs={{0,2},{2,4},{4,6},{6,8},{8,10},{10,12},{12,14},{14,0},{1,3},{3,5},... | collective-permute-start | bytes 294920 | tf_op jit(solution)/shard_map/ppermute | solution.py:96
  28.5 6.0 %collective-permute-start.9 = (bf16[128,384]{1,0:T(8,128)(2,1)S(1)}, bf16[128,384]{1,0:T(8,128)(2,1)S(1)}, u32[]{:S(2)}, u32[]{:S(2)}) collective-permute-start(bf16[128,384]{1,0:T(8,128)(2,1)S(1)} %get-tuple-element.48), channel_id=1, source_target_pairs={{0,14},{2,0},{4,2},{6,4},{8,6},{10,8},{12,10},{14,12},{1,15},{3,1}... | collective-permute-start | bytes 294920 | tf_op jit(solution)/shard_map/ppermute | solution.py:96
  30.8 7.4 %collective-permute-start.6 = (bf16[128,768]{1,0:T(8,128)(2,1)S(1)}, bf16[128,768]{1,0:T(8,128)(2,1)S(1)}, u32[]{:S(2)}, u32[]{:S(2)}) collective-permute-start(bf16[128,768]{1,0:T(8,128)(2,1)S(1)} %pad_maximum_fusion.5), channel_id=1, source_target_pairs={{0,2},{2,4},{4,6},{6,8},{8,10},{10,12},{12,14},{14,0},{1,3},{3,5},... | collective-permute-start | bytes 589832 | tf_op jit(solution)/shard_map/ppermute | solution.py:96
  34.6 7.8 %collective-permute-start.10 = (bf16[128,768]{1,0:T(8,128)(2,1)S(1)}, bf16[128,768]{1,0:T(8,128)(2,1)S(1)}, u32[]{:S(2)}, u32[]{:S(2)}) collective-permute-start(bf16[128,768]{1,0:T(8,128)(2,1)S(1)} %pad_maximum_fusion.6), channel_id=1, source_target_pairs={{0,14},{2,0},{4,2},{6,4},{8,6},{10,8},{12,10},{14,12},{1,15},{3,1}... | collective-permute-start | bytes 589832 | tf_op jit(solution)/shard_map/ppermute | solution.py:96
  38.2 11.6 %collective-permute-start.7 = (bf16[128,768]{1,0:T(8,128)(2,1)S(1)}, bf16[128,768]{1,0:T(8,128)(2,1)S(1)}, u32[]{:S(2)}, u32[]{:S(2)}) collective-permute-start(bf16[128,768]{1,0:T(8,128)(2,1)S(1)} %bitcast_add_fusion.2), channel_id=1, source_target_pairs={{0,2},{2,4},{4,6},{6,8},{8,10},{10,12},{12,14},{14,0},{1,3},{3,5},... | collective-permute-start | bytes 589832 | tf_op jit(solution)/shard_map/ppermute | solution.py:96
  49.8 12.3 %collective-permute-start.11 = (bf16[128,768]{1,0:T(8,128)(2,1)S(1)}, bf16[128,768]{1,0:T(8,128)(2,1)S(1)}, u32[]{:S(2)}, u32[]{:S(2)}) collective-permute-start(bf16[128,768]{1,0:T(8,128)(2,1)S(1)} %get-tuple-element.32), channel_id=1, source_target_pairs={{0,14},{2,0},{4,2},{6,4},{8,6},{10,8},{12,10},{14,12},{1,15},{3,1}... | collective-permute-start | bytes 589832 | tf_op jit(solution)/shard_map/ppermute | solution.py:96
  49.9 12.6 %collective-permute-start.8 = (bf16[128,768]{1,0:T(8,128)(2,1)S(1)}, bf16[128,768]{1,0:T(8,128)(2,1)S(1)}, u32[]{:S(2)}, u32[]{:S(2)}) collective-permute-start(bf16[128,768]{1,0:T(8,128)(2,1)S(1)} %get-tuple-element.31), channel_id=1, source_target_pairs={{0,2},{2,4},{4,6},{6,8},{8,10},{10,12},{12,14},{14,0},{1,3},{3,5},... | collective-permute-start | bytes 589832 | tf_op jit(solution)/shard_map/ppermute | solution.py:96
  62.2 11.6 %collective-permute-start.12 = (bf16[128,768]{1,0:T(8,128)(2,1)S(1)}, bf16[128,768]{1,0:T(8,128)(2,1)S(1)}, u32[]{:S(2)}, u32[]{:S(2)}) collective-permute-start(bf16[128,768]{1,0:T(8,128)(2,1)S(1)} %bitcast_add_fusion.1), channel_id=1, source_target_pairs={{0,14},{2,0},{4,2},{6,4},{8,6},{10,8},{12,10},{14,12},{1,15},{3,1}... | collective-permute-start | bytes 589832 | tf_op jit(solution)/shard_map/ppermute | solution.py:96
  62.5 17.9 %copy-start.3 = (bf16[128,2048]{1,0:T(8,128)(2,1)S(1)}, bf16[128,2048]{1,0:T(8,128)(2,1)}, u32[]{:S(2)}) copy-start(bf16[128,2048]{1,0:T(8,128)(2,1)} %param.19) | copy-start | bytes 1572868
  62.5 17.8 %copy-start.4 = (f32[2048]{0:T(1024)S(1)}, f32[2048]{0:T(1024)}, u32[]{:S(2)}) copy-start(f32[2048]{0:T(1024)} %param.20) | copy-start | bytes 24580
  80.1 0.7 copy-start.5
  102.1 135.2 %reduce-scatter.5.cloned.1.call-start = ((), (), s32[]{:S(2)}) async-start(), calls=%async_computation.7 | async-start | bytes 4128768 | tf_op jit(solution)/shard_map/reduce_scatter | solution.py:348
  103.6 6.8 %collective-permute-start.16 = (bf16[48,2176]{1,0:T(8,128)(2,1)S(1)}, bf16[48,2176]{1,0:T(8,128)(2,1)S(1)}, u32[]{:S(2)}, u32[]{:S(2)}) collective-permute-start(bf16[48,2176]{1,0:T(8,128)(2,1)S(1)} %get-tuple-element.51), channel_id=1, source_target_pairs={{0,2},{2,4},{4,6},{6,8},{8,10},{10,12},{12,14},{14,0},{1,3},{3,5},... | collective-permute-start | bytes 626696 | tf_op jit(solution)/shard_map/ppermute | solution.py:96
  105.1 7.0 %collective-permute-start.17 = (bf16[48,2176]{1,0:T(8,128)(2,1)S(1)}, bf16[48,2176]{1,0:T(8,128)(2,1)S(1)}, u32[]{:S(2)}, u32[]{:S(2)}) collective-permute-start(bf16[48,2176]{1,0:T(8,128)(2,1)S(1)} %get-tuple-element.51), channel_id=1, source_target_pairs={{0,14},{2,0},{4,2},{6,4},{8,6},{10,8},{12,10},{14,12},{1,15},{3,1}... | collective-permute-start | bytes 626696 | tf_op jit(solution)/shard_map/ppermute | solution.py:96
  110.4 11.4 %collective-permute-start.18 = (bf16[48,2176]{1,0:T(8,128)(2,1)S(1)}, bf16[48,2176]{1,0:T(8,128)(2,1)S(1)}, u32[]{:S(2)}, u32[]{:S(2)}) collective-permute-start(bf16[48,2176]{1,0:T(8,128)(2,1)S(1)} %collective-permute-done.16), channel_id=1, source_target_pairs={{0,2},{2,4},{4,6},{6,8},{8,10},{10,12},{12,14},{14,0},{1,3},{3,5},... | collective-permute-start | bytes 626696 | tf_op jit(solution)/shard_map/ppermute | solution.py:96
  112.1 12.4 %collective-permute-start.19 = (bf16[48,2176]{1,0:T(8,128)(2,1)S(1)}, bf16[48,2176]{1,0:T(8,128)(2,1)S(1)}, u32[]{:S(2)}, u32[]{:S(2)}) collective-permute-start(bf16[48,2176]{1,0:T(8,128)(2,1)S(1)} %collective-permute-done.17), channel_id=1, source_target_pairs={{0,14},{2,0},{4,2},{6,4},{8,6},{10,8},{12,10},{14,12},{1,15},{3,1}... | collective-permute-start | bytes 626696 | tf_op jit(solution)/shard_map/ppermute | solution.py:96
  121.8 15.1 %collective-permute-start.20 = (bf16[48,2176]{1,0:T(8,128)(2,1)S(1)}, bf16[48,2176]{1,0:T(8,128)(2,1)S(1)}, u32[]{:S(2)}, u32[]{:S(2)}) collective-permute-start(bf16[48,2176]{1,0:T(8,128)(2,1)S(1)} %collective-permute-done.18), channel_id=1, source_target_pairs={{0,2},{2,4},{4,6},{6,8},{8,10},{10,12},{12,14},{14,0},{1,3},{3,5},... | collective-permute-start | bytes 626696 | tf_op jit(solution)/shard_map/ppermute | solution.py:96
  124.5 12.3 %collective-permute-start.21 = (bf16[48,2176]{1,0:T(8,128)(2,1)S(1)}, bf16[48,2176]{1,0:T(8,128)(2,1)S(1)}, u32[]{:S(2)}, u32[]{:S(2)}) collective-permute-start(bf16[48,2176]{1,0:T(8,128)(2,1)S(1)} %collective-permute-done.19), channel_id=1, source_target_pairs={{0,14},{2,0},{4,2},{6,4},{8,6},{10,8},{12,10},{14,12},{1,15},{3,1}... | collective-permute-start | bytes 626696 | tf_op jit(solution)/shard_map/ppermute | solution.py:96
  136.8 8.5 %collective-permute-start.23 = (bf16[48,1152]{1,0:T(8,128)(2,1)S(1)}, bf16[48,1152]{1,0:T(8,128)(2,1)S(1)}, u32[]{:S(2)}, u32[]{:S(2)}) collective-permute-start(bf16[48,1152]{1,0:T(8,128)(2,1)S(1)} %slice.152), channel_id=1, source_target_pairs={{0,14},{2,0},{4,2},{6,4},{8,6},{10,8},{12,10},{14,12},{1,15},{3,1}... | collective-permute-start | bytes 331784 | tf_op jit(solution)/shard_map/ppermute | solution.py:96
  137.0 7.9 %collective-permute-start.22 = (bf16[48,1024]{1,0:T(8,128)(2,1)S(1)}, bf16[48,1024]{1,0:T(8,128)(2,1)S(1)}, u32[]{:S(2)}, u32[]{:S(2)}) collective-permute-start(bf16[48,1024]{1,0:T(8,128)(2,1)S(1)} %slice.151), channel_id=1, source_target_pairs={{0,2},{2,4},{4,6},{6,8},{8,10},{10,12},{12,14},{14,0},{1,3},{3,5},... | collective-permute-start | bytes 294920 | tf_op jit(solution)/shard_map/ppermute | solution.py:96
  176.5 18.7 %copy-start.1 = (bf16[384,2048]{1,0:T(8,128)(2,1)S(1)}, bf16[384,2048]{1,0:T(8,128)(2,1)}, u32[]{:S(2)}) copy-start(bf16[384,2048]{1,0:T(8,128)(2,1)} %experts.2) | copy-start | bytes 4718596
  177.5 4.6 %collective-permute-start.24 = (bf16[48,1024]{1,0:T(8,128)(2,1)S(1)}, bf16[48,1024]{1,0:T(8,128)(2,1)S(1)}, u32[]{:S(2)}, u32[]{:S(2)}) collective-permute-start(bf16[48,1024]{1,0:T(8,128)(2,1)S(1)} %slice.130), channel_id=1, source_target_pairs={{0,2},{2,4},{4,6},{6,8},{8,10},{10,12},{12,14},{14,0},{1,3},{3,5},... | collective-permute-start | bytes 294920 | tf_op jit(solution)/shard_map/ppermute | solution.py:96
  183.2 7.7 %collective-permute-start.28 = (bf16[48,1024]{1,0:T(8,128)(2,1)S(1)}, bf16[48,1024]{1,0:T(8,128)(2,1)S(1)}, u32[]{:S(2)}, u32[]{:S(2)}) collective-permute-start(bf16[48,1024]{1,0:T(8,128)(2,1)S(1)} %get-tuple-element.28), channel_id=1, source_target_pairs={{0,14},{2,0},{4,2},{6,4},{8,6},{10,8},{12,10},{14,12},{1,15},{3,1}... | collective-permute-start | bytes 294920 | tf_op jit(solution)/shard_map/ppermute | solution.py:96
  183.3 11.9 %collective-permute-start.25 = (bf16[48,2048]{1,0:T(8,128)(2,1)S(1)}, bf16[48,2048]{1,0:T(8,128)(2,1)S(1)}, u32[]{:S(2)}, u32[]{:S(2)}) collective-permute-start(bf16[48,2048]{1,0:T(8,128)(2,1)S(1)} %pad_maximum_fusion.7), channel_id=1, source_target_pairs={{0,2},{2,4},{4,6},{6,8},{8,10},{10,12},{12,14},{14,0},{1,3},{3,5},... | collective-permute-start | bytes 589832 | tf_op jit(solution)/shard_map/ppermute | solution.py:96
  191.9 11.6 %collective-permute-start.29 = (bf16[48,2048]{1,0:T(8,128)(2,1)S(1)}, bf16[48,2048]{1,0:T(8,128)(2,1)S(1)}, u32[]{:S(2)}, u32[]{:S(2)}) collective-permute-start(bf16[48,2048]{1,0:T(8,128)(2,1)S(1)} %pad_maximum_fusion.8), channel_id=1, source_target_pairs={{0,14},{2,0},{4,2},{6,4},{8,6},{10,8},{12,10},{14,12},{1,15},{3,1}... | collective-permute-start | bytes 589832 | tf_op jit(solution)/shard_map/ppermute | solution.py:96
  195.3 12.2 %collective-permute-start.26 = (bf16[48,2048]{1,0:T(8,128)(2,1)S(1)}, bf16[48,2048]{1,0:T(8,128)(2,1)S(1)}, u32[]{:S(2)}, u32[]{:S(2)}) collective-permute-start(bf16[48,2048]{1,0:T(8,128)(2,1)S(1)} %slice_add_fusion.2), channel_id=1, source_target_pairs={{0,2},{2,4},{4,6},{6,8},{8,10},{10,12},{12,14},{14,0},{1,3},{3,5},... | collective-permute-start | bytes 589832 | tf_op jit(solution)/shard_map/ppermute | solution.py:96
  207.5 12.1 %collective-permute-start.30 = (bf16[48,2048]{1,0:T(8,128)(2,1)S(1)}, bf16[48,2048]{1,0:T(8,128)(2,1)S(1)}, u32[]{:S(2)}, u32[]{:S(2)}) collective-permute-start(bf16[48,2048]{1,0:T(8,128)(2,1)S(1)} %get-tuple-element.26), channel_id=1, source_target_pairs={{0,14},{2,0},{4,2},{6,4},{8,6},{10,8},{12,10},{14,12},{1,15},{3,1}... | collective-permute-start | bytes 589832 | tf_op jit(solution)/shard_map/ppermute | solution.py:96
  207.6 12.1 %collective-permute-start.27 = (bf16[48,2048]{1,0:T(8,128)(2,1)S(1)}, bf16[48,2048]{1,0:T(8,128)(2,1)S(1)}, u32[]{:S(2)}, u32[]{:S(2)}) collective-permute-start(bf16[48,2048]{1,0:T(8,128)(2,1)S(1)} %get-tuple-element.25), channel_id=1, source_target_pairs={{0,2},{2,4},{4,6},{6,8},{8,10},{10,12},{12,14},{14,0},{1,3},{3,5},... | collective-permute-start | bytes 589832 | tf_op jit(solution)/shard_map/ppermute | solution.py:96
  219.6 11.6 %collective-permute-start.31 = (bf16[48,2048]{1,0:T(8,128)(2,1)S(1)}, bf16[48,2048]{1,0:T(8,128)(2,1)S(1)}, u32[]{:S(2)}, u32[]{:S(2)}) collective-permute-start(bf16[48,2048]{1,0:T(8,128)(2,1)S(1)} %slice_add_fusion.1), channel_id=1, source_target_pairs={{0,14},{2,0},{4,2},{6,4},{8,6},{10,8},{12,10},{14,12},{1,15},{3,1}... | collective-permute-start | bytes 589832 | tf_op jit(solution)/shard_map/ppermute | solution.py:96
  232.0 13.5 %all-to-all-start.2 = ((bf16[16,48,128]{2,1,0:T(8,128)(2,1)}), bf16[16,48,128]{2,1,0:T(8,128)(2,1)S(1)}, u32[]{:S(2)}, u32[]{:S(2)}) async-start(bf16[16,48,128]{2,1,0:T(8,128)(2,1)} %reshape.167), calls=%async_computation.4 | async-start | bytes 393216 | tf_op jit(solution)/shard_map/all_to_all | solution.py:329
Sparse Core Ops, SparseCore 0:
  23.6 55.3 reduce-scatter.2
  102.2 58.7 all-gather.1
  176.6 60.6 reduce-scatter.4
